TPU v7x, 32 devices: a whole 2x2x4 slice. The times are simulated.
32 devices in a mesh: sp: 8 (over z, core), tp: 4 (over y, x).
Axes of the slice: x: 2, y: 2, z: 4, core: 2. Of those that a mesh axis runs over, the one named last changes fastest.
Arguments:
- query_rows: bfloat16 [4096, 1024], P('sp', 'tp'), may hold values from -128 to 128
- key_rows: bfloat16 [4096, 1024], P('sp', 'tp'), may hold values from -4 to 4
- value_rows: bfloat16 [4096, 1024], P('sp', 'tp'), may hold values from -6 to 6
- cum_gates: float32 [4096, 16], P('sp', 'tp'), may hold values from -4098 to 0, as said below
- residual: bfloat16 [4096, 2048], P('sp', 'tp'), may hold values from -64 to 64
- output_weight: bfloat16 [1024, 2048], P(None, 'tp'), may hold values from -0.1875 to 0.1875
- norm_gain: bfloat16 [2048], replicated, may hold values from 0.099609375 to 1.8984375
- expert_index: int32 [4096, 2], P('sp'), may hold values from 0 to 7, all different within a row; in each aligned block of 512 rows (0 to 511, 512 to 1023, ...) at most 256 rows name the same one
- route_weights: float32 [4096, 2], P('sp'), may hold values from 0.2 to 1
- gate_weight: bfloat16 [8, 2048, 2048], P('sp', None, 'tp'), may hold values from -2 to 2
- up_weight: bfloat16 [8, 2048, 2048], P('sp', None, 'tp'), may hold values from -2 to 2
- down_weight: bfloat16 [8, 2048, 2048], P('sp', None, 'tp'), may hold values from -0.125 to 0.125
Outputs:
- layer_out: bfloat16 [4096, 2048], P('sp', 'tp')
Inputs may be any that keep to these rules, and one draw needn't show every extreme that they name: `cum_gates`: each head's values never rise along positions. `expert_index`: each token names 2 different experts. In the 512 tokens of one index of sp no expert is named more than 256 times, and in some index's tokens some expert is named exactly 256 times.
All inputs are finite; a program needn't handle non-finite values.
Results may differ from a plain program's by a relative error of at most 0.01.
Values may be sent and summed in bfloat16 or wider, within the bound.
A program may use at most 64 MiB of HBM per device.

v0:
```python
import functools
import math

import jax
import jax.numpy as jnp
from jax import lax
from jax.experimental import pallas as pl
from jax.experimental.pallas import tpu as pltpu
from jax.sharding import PartitionSpec as P

NORM_EPS = 1e-06
CLAMP_LIMIT = 7.0
SILU_ALPHA = 1.702
CHUNKS = 1


def normalize(rows, norm_gain):
    wide = rows.astype(jnp.float32)
    factor = lax.rsqrt(jnp.mean(wide * wide, axis=-1, keepdims=True) + NORM_EPS)
    return (wide * factor * norm_gain.astype(jnp.float32)).astype(jnp.bfloat16)


def attend_kernel(heads, q_ref, kv_ref, gates_ref, out_ref, masked_q, top, total, summed):
    rows, width = q_ref.shape
    head_size = width // heads
    lanes = min(width, 128)
    tile = math.gcd(rows, 256)
    tiles = rows // tile
    me = lax.axis_index("sp")
    scale = head_size ** (-0.5)
    lane = lax.broadcasted_iota(jnp.int32, (rows, lanes), 1)
    for h in range(heads):
        group, inside = divmod(h * head_size, lanes)
        part = q_ref[:, group * lanes : (group + 1) * lanes].astype(jnp.float32) * scale
        keep = (lane >= inside) & (lane < inside + head_size)
        masked_q[h] = jnp.where(keep, part, 0.0).astype(jnp.bfloat16)
    top[...] = jnp.full(top.shape, -1e30, jnp.float32)
    total[...] = jnp.zeros(total.shape, jnp.float32)
    summed[...] = jnp.zeros(summed.shape, jnp.float32)

    def block(number, diagonal):
        base = pl.multiple_of(number * rows, rows)
        for h in range(heads):
            group = h * head_size // lanes
            keys = kv_ref[pl.ds(base, rows), group * lanes : (group + 1) * lanes]
            values = kv_ref[pl.ds(base, rows), width + group * lanes : width + (group + 1) * lanes]
            gates = gates_ref[number, h : h + 1, :]
            for t in range(tiles):
                span = slice(t * tile, (t + 1) * tile)
                count = (t + 1) * tile if diagonal else rows
                scores = lax.dot_general(
                    masked_q[h, span],
                    keys[:count],
                    (((1,), (1,)), ((), ())),
                    preferred_element_type=jnp.float32,
                )
                scores = scores - gates[:, :count]
                if diagonal:
                    row = lax.broadcasted_iota(jnp.int32, (tile, count), 0) + t * tile
                    col = lax.broadcasted_iota(jnp.int32, (tile, count), 1)
                    scores = jnp.where(col <= row, scores, -jnp.inf)
                old = top[h, span]
                new = jnp.maximum(old, jnp.max(scores, axis=1, keepdims=True))
                raised = jnp.exp(scores - new[:, :1])
                shrink = jnp.exp(old - new)
                part = raised[:, :128]
                for c in range(128, count, 128):
                    part = part + raised[:, c : c + 128]
                top[h, span] = new
                total[h, span] = total[h, span] * shrink + part
                product = lax.dot_general(
                    raised.astype(jnp.bfloat16),
                    values[:count],
                    (((1,), (0,)), ((), ())),
                    preferred_element_type=jnp.float32,
                )
                summed[h, span] = summed[h, span] * shrink[:, :lanes] + product

    def step(number, carry):
        block(number, False)
        return carry

    lax.fori_loop(0, me, step, 0)
    block(me, True)
    for g in range(width // lanes):
        result = jnp.zeros((rows, lanes), jnp.float32)
        for h in range(heads):
            if h * head_size // lanes == g:
                inside = h * head_size % lanes
                keep = (lane >= inside) & (lane < inside + head_size)
                whole = jnp.sum(total[h], axis=1, keepdims=True)
                result = jnp.where(keep, summed[h] / whole, result)
        out_ref[:, g * lanes : (g + 1) * lanes] = result.astype(out_ref.dtype)


def attend_local(query_rows, kv_all, gates_all):
    rows, width = query_rows.shape
    groups, heads, _ = gates_all.shape
    lanes = min(width, 128)
    return pl.pallas_call(
        functools.partial(attend_kernel, heads),
        out_shape=jax.ShapeDtypeStruct((rows, width), jnp.bfloat16),
        in_specs=[pl.BlockSpec(memory_space=pltpu.VMEM)] * 3,
        out_specs=pl.BlockSpec(memory_space=pltpu.VMEM),
        scratch_shapes=[
            pltpu.VMEM((heads, rows, lanes), jnp.bfloat16),
            pltpu.VMEM((heads, rows, 128), jnp.float32),
            pltpu.VMEM((heads, rows, 128), jnp.float32),
            pltpu.VMEM((heads, rows, lanes), jnp.float32),
        ],
        compiler_params=pltpu.CompilerParams(vmem_limit_bytes=48 * 2**20),
        cost_estimate=pl.CostEstimate(
            flops=4 * rows * rows * groups * width * 4,
            bytes_accessed=4 * rows * groups * width,
            transcendentals=rows * rows * groups * heads,
        ),
    )(query_rows, kv_all, gates_all)


def experts_kernel(
    groups,
    mixed_ref,
    place_row_ref,
    place_col_ref,
    route_ref,
    gain_ref,
    gate_ref,
    up_ref,
    down_ref,
    out_ref,
    outbox,
    full,
    act,
    made,
    returned,
    total,
    out_send,
    out_recv,
    one_send,
    one_recv,
    two_send,
    two_recv,
    back_send,
    back_recv,
):
    topk = route_ref.shape[1]
    rows = mixed_ref.shape[0]
    capacity, columns = outbox.shape[1:]
    half = capacity // 2
    shards = full.shape[1]
    sp = lax.axis_index("sp")
    tp = lax.axis_index("tp")
    beside = tp + 1 - 2 * (tp % 2)
    across = (tp + 2) % 4

    def partner(number):
        found, bit = 0, 1
        while bit < groups:
            found = found + bit * (((sp // bit) % 2 + (number // bit) % 2) % 2)
            bit *= 2
        return found

    def send(src, dst, send_sem, recv_sem, device):
        return pltpu.make_async_remote_copy(
            src_ref=src,
            dst_ref=dst,
            send_sem=send_sem,
            recv_sem=recv_sem,
            device_id=device,
            device_id_type=pl.DeviceIdType.MESH,
        )

    def dispatch(i):
        return send(
            outbox.at[i], full.at[i, tp], out_send.at[i], out_recv.at[i], (partner(i), tp)
        )

    def give_back(i):
        return send(made.at[i], returned.at[i], back_send.at[i], back_recv.at[i], (partner(i), tp))

    def direct(i, held, send_sem, recv_sem, which):
        device = (sp, beside if which == 0 else across)
        return send(
            held.at[i, tp], held.at[i, tp], send_sem.at[i, which], recv_sem.at[i, which], device
        )

    def relay(i, held, send_sem, recv_sem, which):
        owner = beside if which == 0 else across
        device = (sp, across if which == 0 else beside)
        part = held.at[i, owner, pl.ds(which * half, half)]
        return send(part, part, send_sem.at[i, 2 + which], recv_sem.at[i, 2 + which], device)

    barrier = pltpu.get_barrier_semaphore()
    for i in range(1, groups):
        pl.semaphore_signal(
            barrier, inc=1, device_id=(partner(i), tp), device_id_type=pl.DeviceIdType.MESH
        )
    for other in (beside, across):
        pl.semaphore_signal(
            barrier, inc=1, device_id=(sp, other), device_id_type=pl.DeviceIdType.MESH
        )
    pl.semaphore_wait(barrier, groups + 1)

    def rows_for(i):
        numbers = lax.broadcasted_iota(jnp.int32, (capacity, rows), 0) + i * capacity
        taken = numbers == place_row_ref[0:1, :]
        for k in range(1, topk):
            taken = taken | (numbers == place_row_ref[k : k + 1, :])
        return jnp.dot(
            jnp.where(taken, 1.0, 0.0).astype(jnp.bfloat16),
            mixed_ref[...],
            preferred_element_type=jnp.float32,
        ).astype(jnp.bfloat16)

    full[0, tp] = rows_for(0)

    def fill(i, carry):
        outbox[i] = rows_for(i)
        dispatch(i).start()
        return carry

    lax.fori_loop(1, groups, fill, 0)
    total[...] = mixed_ref[...].astype(jnp.float32)

    def start_gather(i, held, send_sem, recv_sem):
        direct(i, held, send_sem, recv_sem, 0).start()
        direct(i, held, send_sem, recv_sem, 1).start()

    def pass_on(i, held, send_sem, recv_sem):
        for which in range(2):
            direct(i, held, send_sem, recv_sem, which).wait_recv()
            relay(i, held, send_sem, recv_sem, which).start()

    def finish_gather(i, held, send_sem, recv_sem):
        for which in range(2):
            relay(i, held, send_sem, recv_sem, which).wait_recv()

    def hidden(i):
        square = jnp.zeros((capacity, 1), jnp.float32)
        for j in range(shards):
            wide = full[i, j].astype(jnp.float32)
            square = square + jnp.sum(wide * wide, axis=1, keepdims=True)
        factor = lax.rsqrt(square / (shards * columns) + NORM_EPS)
        gate_input = jnp.zeros((capacity, gate_ref.shape[1]), jnp.float32)
        linear_input = gate_input
        for j in range(shards):
            span = slice(j * columns, (j + 1) * columns)
            gain = gain_ref[0:1, span].astype(jnp.float32)
            normed = (full[i, j].astype(jnp.float32) * factor * gain).astype(jnp.bfloat16)
            gate_input = gate_input + jnp.dot(
                normed, gate_ref[span, :], preferred_element_type=jnp.float32
            )
            linear_input = linear_input + jnp.dot(
                normed, up_ref[span, :], preferred_element_type=jnp.float32
            )
        gate_cut = jnp.minimum(gate_input, CLAMP_LIMIT)
        linear_cut = jnp.clip(linear_input, -CLAMP_LIMIT, CLAMP_LIMIT)
        act[i, tp] = (gate_cut * jax.nn.sigmoid(SILU_ALPHA * gate_cut) * (linear_cut + 1.0)).astype(
            jnp.bfloat16
        )

    def output_rows(i):
        units = act.shape[3]
        result = jnp.zeros((capacity, columns), jnp.float32)
        for j in range(shards):
            result = result + jnp.dot(
                act[i, j],
                down_ref[j * units : (j + 1) * units, :],
                preferred_element_type=jnp.float32,
            )
        return result.astype(jnp.bfloat16)

    def step(i, carry):
        @pl.when(i < groups)
        def _():
            @pl.when(i > 0)
            def _():
                dispatch(i).wait_recv()

            start_gather(i, full, one_send, one_recv)

        @pl.when((i >= 1) & (i < groups + 1))
        def _():
            pass_on(i - 1, full, one_send, one_recv)

        @pl.when((i >= 2) & (i < groups + 2))
        def _():
            finish_gather(i - 2, full, one_send, one_recv)
            hidden(i - 2)
            start_gather(i - 2, act, two_send, two_recv)

        @pl.when((i >= 3) & (i < groups + 3))
        def _():
            pass_on(i - 3, act, two_send, two_recv)

        @pl.when((i >= 4) & (i < groups + 4))
        def _():
            b = i - 4
            finish_gather(b, act, two_send, two_recv)
            result = output_rows(b)

            @pl.when(b == 0)
            def _():
                returned[0] = result

            @pl.when(b > 0)
            def _():
                made[b] = result
                give_back(b).start()

        @pl.when(i >= 5)
        def _():
            b = i - 5

            @pl.when(b > 0)
            def _():
                give_back(b).wait_recv()

            numbers = lax.broadcasted_iota(jnp.int32, (rows, capacity), 1) + b * capacity
            added = total[...]
            for k in range(topk):
                taken = jnp.where(numbers == place_col_ref[:, k : k + 1], 1.0, 0.0)
                picked = jnp.dot(
                    taken.astype(jnp.bfloat16), returned[b], preferred_element_type=jnp.float32
                )
                added = added + route_ref[:, k : k + 1] * picked
            total[...] = added

        return carry

    lax.fori_loop(0, groups + 5, step, 0)
    out_ref[...] = total[...].astype(out_ref.dtype)

    def settle(i, carry):
        @pl.when(i > 0)
        def _():
            dispatch(i).wait_send()
            give_back(i).wait_send()

        for which in range(2):
            direct(i, full, one_send, one_recv, which).wait_send()
            relay(i, full, one_send, one_recv, which).wait_send()
            direct(i, act, two_send, two_recv, which).wait_send()
            relay(i, act, two_send, two_recv, which).wait_send()
        return carry

    lax.fori_loop(0, groups, settle, 0)


def experts_fused(
    mixed, place_row, place_col, route_weights, norm_gain, gate_weight, up_weight, down_weight, capacity
):
    rows, columns = mixed.shape
    groups = lax.axis_size("sp")
    shards = lax.axis_size("tp")
    units = gate_weight.shape[2]
    dma = pltpu.SemaphoreType.DMA
    return pl.pallas_call(
        functools.partial(experts_kernel, groups),
        out_shape=jax.ShapeDtypeStruct((rows, columns), jnp.bfloat16),
        in_specs=[pl.BlockSpec(memory_space=pltpu.VMEM)] * 8,
        out_specs=pl.BlockSpec(memory_space=pltpu.VMEM),
        scratch_shapes=[
            pltpu.VMEM((groups, capacity, columns), jnp.bfloat16),
            pltpu.VMEM((groups, shards, capacity, columns), jnp.bfloat16),
            pltpu.VMEM((groups, shards, capacity, units), jnp.bfloat16),
            pltpu.VMEM((groups, capacity, columns), jnp.bfloat16),
            pltpu.VMEM((groups, capacity, columns), jnp.bfloat16),
            pltpu.VMEM((rows, columns), jnp.float32),
            dma((groups,)),
            dma((groups,)),
            dma((groups, 4)),
            dma((groups, 4)),
            dma((groups, 4)),
            dma((groups, 4)),
            dma((groups,)),
            dma((groups,)),
        ],
        compiler_params=pltpu.CompilerParams(
            collective_id=1, has_side_effects=True, vmem_limit_bytes=56 * 2**20
        ),
    )(
        mixed,
        place_row,
        place_col,
        route_weights,
        norm_gain.reshape(1, -1),
        gate_weight[0],
        up_weight[0],
        down_weight[0],
    )


def mix_kernel(
    heads,
    groups,
    q_ref,
    k_ref,
    v_ref,
    gates_ref,
    weight_ref,
    residual_ref,
    index_row_ref,
    index_col_ref,
    out_ref,
    place_row_ref,
    place_col_ref,
    keys_all,
    values_all,
    gates_all,
    masked_q,
    top,
    total,
    summed,
    attended,
    next_send,
    next_recv,
    side_send,
    side_recv,
    tp_send,
    tp_recv,
):
    rows, width = q_ref.shape
    head_size = width // heads
    lanes = min(width, 128)
    tile = math.gcd(rows, 256)
    tiles = rows // tile
    sp = lax.axis_index("sp")
    tp = lax.axis_index("tp")
    chip = sp // 2
    core = sp % 2
    chips = groups // 2
    sibling = sp + 1 - 2 * core
    beside = tp + 1 - 2 * (tp % 2)
    across = (tp + 2) % 4
    mesh_id = pl.DeviceIdType.MESH
    scale = head_size ** (-0.5)

    def copies(number, own, device, send_sem, recv_sem):
        made = []
        for n, (mine, held) in enumerate(
            ((k_ref, keys_all), (v_ref, values_all), (gates_ref, gates_all))
        ):
            made.append(
                pltpu.make_async_remote_copy(
                    src_ref=mine if own else held.at[number],
                    dst_ref=held.at[number],
                    send_sem=send_sem.at[number, n],
                    recv_sem=recv_sem.at[number, n],
                    device_id=device,
                    device_id_type=mesh_id,
                )
            )
        return made

    def onward(number, own=False):
        return copies(number, own, ((sp + 2) % groups, tp), next_send, next_recv)

    def sideways(number, own=False):
        return copies(number, own, (sibling, tp), side_send, side_recv)

    def direct(which):
        return pltpu.make_async_remote_copy(
            src_ref=attended.at[tp],
            dst_ref=attended.at[tp],
            send_sem=tp_send.at[which],
            recv_sem=tp_recv.at[which],
            device_id=(sp, beside if which == 0 else across),
            device_id_type=mesh_id,
        )

    def relay(which):
        owner = beside if which == 0 else across
        part = attended.at[owner, pl.ds(which * (rows // 2), rows // 2)]
        return pltpu.make_async_remote_copy(
            src_ref=part,
            dst_ref=part,
            send_sem=tp_send.at[2 + which],
            recv_sem=tp_recv.at[2 + which],
            device_id=(sp, across if which == 0 else beside),
            device_id_type=mesh_id,
        )

    barrier = pltpu.get_barrier_semaphore()
    for device in (
        ((sp + 2) % groups, tp),
        ((sp + groups - 2) % groups, tp),
        (sibling, tp),
        (sp, beside),
        (sp, across),
    ):
        pl.semaphore_signal(barrier, inc=1, device_id=device, device_id_type=mesh_id)
    pl.semaphore_wait(barrier, 5)

    @pl.when(chip < chips - 1)
    def _():
        for copy in onward(sp, True):
            copy.start()

    @pl.when(core == 0)
    def _():
        for copy in sideways(sp, True):
            copy.start()

    capacity = 2 * rows * index_row_ref.shape[0] // groups
    topk = index_row_ref.shape[0]
    first = lax.broadcasted_iota(jnp.int32, (rows, rows), 0)
    second = lax.broadcasted_iota(jnp.int32, (rows, rows), 1)
    number = lax.broadcasted_iota(jnp.int32, (rows, 128), 1)
    named = jnp.zeros((rows, 128), jnp.float32)
    for k in range(topk):
        named = named + jnp.where(number == index_col_ref[:, k : k + 1], 1.0, 0.0)
    before = jnp.dot(
        jnp.where(second < first, 1.0, 0.0).astype(jnp.bfloat16),
        named.astype(jnp.bfloat16),
        preferred_element_type=jnp.float32,
    )
    for k in range(topk):
        expert = index_col_ref[:, k : k + 1]
        rank = jnp.sum(jnp.where(number == expert, before, 0.0), axis=1, keepdims=True)
        place_col_ref[:, k : k + 1] = expert * capacity + rank.astype(jnp.int32)
    number = lax.broadcasted_iota(jnp.int32, (128, rows), 0)
    named = jnp.zeros((128, rows), jnp.float32)
    for k in range(topk):
        named = named + jnp.where(number == index_row_ref[k : k + 1, :], 1.0, 0.0)
    before = jnp.dot(
        named.astype(jnp.bfloat16),
        jnp.where(first < second, 1.0, 0.0).astype(jnp.bfloat16),
        preferred_element_type=jnp.float32,
    )
    for k in range(topk):
        expert = index_row_ref[k : k + 1, :]
        rank = jnp.sum(jnp.where(number == expert, before, 0.0), axis=0, keepdims=True)
        place_row_ref[k : k + 1, :] = expert * capacity + rank.astype(jnp.int32)

    lane = lax.broadcasted_iota(jnp.int32, (rows, lanes), 1)
    for h in range(heads):
        group, inside = divmod(h * head_size, lanes)
        part = q_ref[:, group * lanes : (group + 1) * lanes].astype(jnp.float32) * scale
        keep = (lane >= inside) & (lane < inside + head_size)
        masked_q[h] = jnp.where(keep, part, 0.0).astype(jnp.bfloat16)
    top[...] = jnp.full(top.shape, -1e30, jnp.float32)
    total[...] = jnp.zeros(total.shape, jnp.float32)
    summed[...] = jnp.zeros(summed.shape, jnp.float32)

    def block(key_block, value_block, gate_block, diagonal):
        for h in range(heads):
            group = h * head_size // lanes
            keys = key_block[:, group * lanes : (group + 1) * lanes]
            values = value_block[:, group * lanes : (group + 1) * lanes]
            gates = gate_block[h : h + 1, :]
            for t in range(tiles):
                span = slice(t * tile, (t + 1) * tile)
                count = (t + 1) * tile if diagonal else rows
                scores = lax.dot_general(
                    masked_q[h, span],
                    keys[:count],
                    (((1,), (1,)), ((), ())),
                    preferred_element_type=jnp.float32,
                )
                scores = scores - gates[:, :count]
                if diagonal:
                    row = lax.broadcasted_iota(jnp.int32, (tile, count), 0) + t * tile
                    col = lax.broadcasted_iota(jnp.int32, (tile, count), 1)
                    scores = jnp.where(col <= row, scores, -jnp.inf)
                old = top[h, span]
                new = jnp.maximum(old, jnp.max(scores, axis=1, keepdims=True))
                raised = jnp.exp(scores - new[:, :1])
                shrink = jnp.exp(old - new)
                part = raised[:, :128]
                for c in range(128, count, 128):
                    part = part + raised[:, c : c + 128]
                top[h, span] = new
                total[h, span] = total[h, span] * shrink + part
                product = lax.dot_general(
                    raised.astype(jnp.bfloat16),
                    values[:count],
                    (((1,), (0,)), ((), ())),
                    preferred_element_type=jnp.float32,
                )
                summed[h, span] = summed[h, span] * shrink[:, :lanes] + product

    block(k_ref, v_ref, gates_ref, True)

    def step(d, carry):
        mine = sp - 2 * (d // 2)
        other = sibling - 2 * (d // 2)

        @pl.when((d % 2 == 0) & (d >= 2))
        def _():
            for copy in onward(mine):
                copy.wait_recv()

            @pl.when(chip < chips - 1)
            def _():
                for copy in onward(mine):
                    copy.start()

            for copy in sideways(mine):
                copy.start()

        @pl.when(d % 2 == 1)
        def _():
            for copy in sideways(other):
                copy.wait_recv()

        now = mine * (1 - d % 2) + other * (d % 2)
        block(keys_all.at[now], values_all.at[now], gates_all.at[now], False)
        return carry

    lax.fori_loop(2 - core, 2 * chip + 2, step, 0)

    for g in range(width // lanes):
        result = jnp.zeros((rows, lanes), jnp.float32)
        for h in range(heads):
            if h * head_size // lanes == g:
                inside = h * head_size % lanes
                keep = (lane >= inside) & (lane < inside + head_size)
                whole = jnp.sum(total[h], axis=1, keepdims=True)
                result = jnp.where(keep, summed[h] / whole, result)
        attended[tp, :, g * lanes : (g + 1) * lanes] = result.astype(jnp.bfloat16)
    direct(0).start()
    direct(1).start()

    def projected(owner):
        return jnp.dot(
            attended[owner],
            weight_ref[pl.ds(pl.multiple_of(owner * width, width), width), :],
            preferred_element_type=jnp.float32,
        )

    mixed = residual_ref[...].astype(jnp.float32) + projected(tp)
    for which, owner in ((0, beside), (1, across)):
        direct(which).wait_recv()
        relay(which).start()
        mixed = mixed + projected(owner)
    relay(0).wait_recv()
    relay(1).wait_recv()
    out_ref[...] = (mixed + projected((beside + 2) % 4)).astype(out_ref.dtype)

    for which in range(2):
        direct(which).wait_send()
        relay(which).wait_send()

    @pl.when(chip < chips - 1)
    def _():
        for copy in onward(sp, True):
            copy.wait_send()

    @pl.when(core == 0)
    def _():
        for copy in sideways(sp, True):
            copy.wait_send()

    def settle(d, carry):
        @pl.when(chip < chips - 1)
        def _():
            for copy in onward(sp - 2 * d):
                copy.wait_send()

        for copy in sideways(sp - 2 * d):
            copy.wait_send()
        return carry

    lax.fori_loop(1, chip + 1, settle, 0)


def mix_fused(query_rows, key_rows, value_rows, gates, output_weight, residual, index):
    rows, width = query_rows.shape
    heads = gates.shape[0]
    groups = lax.axis_size("sp")
    lanes = min(width, 128)
    dma = pltpu.SemaphoreType.DMA
    return pl.pallas_call(
        functools.partial(mix_kernel, heads, groups),
        out_shape=(
            jax.ShapeDtypeStruct(residual.shape, jnp.bfloat16),
            jax.ShapeDtypeStruct(index.shape[::-1], jnp.int32),
            jax.ShapeDtypeStruct(index.shape, jnp.int32),
        ),
        in_specs=[pl.BlockSpec(memory_space=pltpu.VMEM)] * 8,
        out_specs=(pl.BlockSpec(memory_space=pltpu.VMEM),) * 3,
        scratch_shapes=[
            pltpu.VMEM((groups, rows, width), jnp.bfloat16),
            pltpu.VMEM((groups, rows, width), jnp.bfloat16),
            pltpu.VMEM((groups, heads, rows), jnp.float32),
            pltpu.VMEM((heads, rows, lanes), jnp.bfloat16),
            pltpu.VMEM((heads, rows, 128), jnp.float32),
            pltpu.VMEM((heads, rows, 128), jnp.float32),
            pltpu.VMEM((heads, rows, lanes), jnp.float32),
            pltpu.VMEM((4, rows, width), jnp.bfloat16),
            dma((groups, 3)),
            dma((groups, 3)),
            dma((groups, 3)),
            dma((groups, 3)),
            dma((4,)),
            dma((4,)),
        ],
        compiler_params=pltpu.CompilerParams(
            collective_id=2, has_side_effects=True, vmem_limit_bytes=40 * 2**20
        ),
    )(query_rows, key_rows, value_rows, gates, output_weight, residual, index.T, index)


def body(
    query_rows,
    key_rows,
    value_rows,
    cum_gates,
    residual,
    output_weight,
    norm_gain,
    expert_index,
    route_weights,
    gate_weight,
    up_weight,
    down_weight,
):
    rows, columns = residual.shape
    topk = expert_index.shape[1]
    local_experts = gate_weight.shape[0]
    groups = lax.axis_size("sp")
    experts = local_experts * groups
    capacity = 2 * rows * topk // experts
    heads = cum_gates.shape[1]

    if lax.axis_size("tp") == 4 and local_experts == 1 and groups in (4, 8):
        index = expert_index ^ lax.axis_index("sp")
        mixed, place_row, place_col = mix_fused(
            query_rows, key_rows, value_rows, cum_gates.T, output_weight, residual, index
        )
        return experts_fused(
            mixed,
            place_row,
            place_col,
            route_weights,
            norm_gain,
            gate_weight,
            up_weight,
            down_weight,
            capacity,
        )

    both = jnp.concatenate([key_rows, value_rows], axis=1)
    kv_all = lax.all_gather(both, "sp", axis=0, tiled=True)
    gates_all = lax.all_gather(cum_gates.T, "sp", axis=0, tiled=False)

    chosen = expert_index.reshape(rows * topk)
    matches = (chosen[:, None] == jnp.arange(experts, dtype=jnp.int32)[None, :]).astype(jnp.int32)
    rank = jnp.sum((jnp.cumsum(matches, axis=0) - matches) * matches, axis=1)
    chosen, rank, gates_all = lax.optimization_barrier((chosen, rank, gates_all))

    attended = attend_local(query_rows, kv_all, gates_all)
    projected = jnp.dot(
        lax.all_gather(attended, "tp", axis=1, tiled=True),
        output_weight,
        preferred_element_type=jnp.float32,
    )
    mixed = (residual.astype(jnp.float32) + projected).astype(jnp.bfloat16)

    chunks = math.gcd(capacity, CHUNKS)
    piece = capacity // chunks
    places = chosen * piece + rank % piece
    inside = rank // piece
    blended = jnp.zeros((rows, columns), jnp.float32)
    for c in range(chunks):
        place = jnp.where(inside == c, places, -1).reshape(rows, topk)
        numbers = jnp.arange(experts * piece, dtype=jnp.int32)
        taken = numbers[:, None] == place[:, 0][None, :]
        for k in range(1, topk):
            taken = taken | (numbers[:, None] == place[:, k][None, :])
        outgoing = jnp.dot(
            taken.astype(jnp.bfloat16), mixed, preferred_element_type=jnp.float32
        ).astype(jnp.bfloat16)
        arrived = lax.all_to_all(
            outgoing.reshape(experts, piece, columns), "sp", split_axis=0, concat_axis=0, tiled=True
        )
        grouped = arrived.reshape(groups, local_experts, piece, columns)
        normed = normalize(lax.all_gather(grouped, "tp", axis=3, tiled=True), norm_gain)
        gate_input = jnp.einsum(
            "seid,edf->seif", normed, gate_weight, preferred_element_type=jnp.float32
        )
        linear_input = jnp.einsum(
            "seid,edf->seif", normed, up_weight, preferred_element_type=jnp.float32
        )
        gate_cut = jnp.minimum(gate_input, CLAMP_LIMIT)
        linear_cut = jnp.clip(linear_input, -CLAMP_LIMIT, CLAMP_LIMIT)
        activated = (gate_cut * jax.nn.sigmoid(SILU_ALPHA * gate_cut) * (linear_cut + 1.0)).astype(
            jnp.bfloat16
        )
        produced = jnp.einsum(
            "seif,efc->seic",
            lax.all_gather(activated, "tp", axis=3, tiled=True),
            down_weight,
            preferred_element_type=jnp.float32,
        ).astype(jnp.bfloat16)
        returned = lax.all_to_all(
            produced.reshape(experts, piece, columns), "sp", split_axis=0, concat_axis=0, tiled=True
        ).reshape(experts * piece, columns)
        for k in range(topk):
            picked = jnp.dot(
                (place[:, k][:, None] == numbers[None, :]).astype(jnp.bfloat16),
                returned,
                preferred_element_type=jnp.float32,
            )
            blended = blended + route_weights[:, k : k + 1] * picked
    return (mixed.astype(jnp.float32) + blended).astype(jnp.bfloat16)


def solution(mesh):
    placed = (
        P("sp", "tp"),
        P("sp", "tp"),
        P("sp", "tp"),
        P("sp", "tp"),
        P("sp", "tp"),
        P(None, "tp"),
        P(),
        P("sp", None),
        P("sp", None),
        P("sp", None, "tp"),
        P("sp", None, "tp"),
        P("sp", None, "tp"),
    )
    return jax.shard_map(body, mesh=mesh, in_specs=placed, out_specs=P("sp", "tp"), check_vma=False)
```

profile of v0, /device:TPU:17, one launch (start us, length us, event | category | flops | bytes accessed | tf_op | source)
XLA Modules:
  0.0 242.3 jit_solution(6815681115265317283)
XLA Ops:
  0.0 0.0 copy-start
  0.0 0.0 copy-start.1
  0.0 1.4 reshape.3.gain_ref
  1.4 0.8 copy.13
  2.3 0.1 copy.14.index_row_ref
  2.4 1.5 copy.15.route_ref
  4.0 0.0 copy-done
  4.0 0.0 copy-done.1
  4.0 0.0 copy-start.3
  4.0 0.9 copy-done.3
  4.9 0.0 copy-start.4
  4.9 0.9 copy-done.4
  5.9 0.0 copy-start.5
  5.9 0.9 copy-done.5
  6.8 0.0 copy-start.7
  6.8 0.7 copy-done.7
  7.5 44.4 %shard_map.118 = (bf16[512,512]{1,0:T(8,128)(2,1)S(1)}, s32[2,512]{1,0:T(2,128)S(1)}, s32[512,2]{1,0:T(8,128)S(1)}) custom-call(bf16[512,256]{1,0:T(8,128)(2,1)S(1)} %copy-done.3, bf16[512,256]{1,0:T(8,128)(2,1)S(1)} %copy-done.4, bf16[512,256]{1,0:T(8,128)(2,1)S(1)} %copy-done.5, f32[4,512]{1,0:T(4,128)S(1)} %bitcast.6, bf16[1024,512]{1,0:T(8,128)(2,1)S(1)} %copy-done, ...), custom_call_target="tpu_custom_call" | custom-call | tf_op jit(solution)/shard_map/pallas_call | solution.py:674
  51.9 0.0 copy-start.2
  51.9 0.8 copy-done.2
  52.7 0.0 copy-start.6
  52.7 0.7 copy-done.6
  53.4 0.0 copy-start.8
  53.4 0.6 copy-done.8
  54.0 186.4 %shard_map.119 = bf16[512,512]{1,0:T(8,128)(2,1)} custom-call(bf16[512,512]{1,0:T(8,128)(2,1)} %copy-done.2, s32[2,512]{1,0:T(2,128)} %copy-done.8, s32[512,2]{1,0:T(8,128)} %copy-done.6, f32[512,2]{1,0:T(8,128)} %copy.15.route_ref, bf16[1,2048]{1,0:T(2,128)(2,1)} %reshape.3.gain_ref, bf16[2048,512]{1,0:T(8,128)(2,1)} %bitcast.7, bf16[2048,512]{1,0:T(8,128)(2,1)} %bitcast.8, ...), custom_call_target="tpu_custom_call" | custom-call | tf_op jit(solution)/shard_map/pallas_call | solution.py:358
  240.4 1.9 copy.17
  (2 shorter events, 0.1 us)
Async XLA Ops:
  0.0 4.0 %copy-start = (bf16[1024,512]{1,0:T(8,128)(2,1)S(1)}, bf16[1024,512]{1,0:T(8,128)(2,1)}, u32[]{:S(2)}) copy-start(bf16[1024,512]{1,0:T(8,128)(2,1)} %weight_ref.1) | copy-start | bytes 3145732
  0.0 4.0 %copy-start.1 = (bf16[512,512]{1,0:T(8,128)(2,1)S(1)}, bf16[512,512]{1,0:T(8,128)(2,1)}, u32[]{:S(2)}) copy-start(bf16[512,512]{1,0:T(8,128)(2,1)} %residual_ref.1) | copy-start | bytes 1572868
  4.0 1.0 copy-start.3
  4.9 0.9 copy-start.4
  5.9 0.9 copy-start.5
  6.8 0.7 copy-start.7
  51.9 0.8 copy-start.2
  52.7 0.7 copy-start.6
  53.4 0.6 copy-start.8
where the time goes:
time: 243 us; the launch traced here: 242 us
  Pallas kernels  231 us (95%)
  local copies, waits for them, and re-layouts  11.4 us (5%)
    pallas_call x1, Pallas kernels, experts_fused(): pl.pallas_call(functools.partial(experts_kernel, groups), out_shape=jax.S...  186 us
    pallas_call x1, Pallas kernels, mix_fused(): pl.pallas_call(functools.partial(mix_kernel, heads, groups), out_shape=(j...  44.4 us
    unnamed x21, local copies, waits for them, and re-layouts  9.86 us

commit v1 on v0

--- a/solution.py
+++ b/solution.py
@@ -117,281 +117,15 @@
     )(query_rows, kv_all, gates_all)
 
 
-def experts_kernel(
-    groups,
-    mixed_ref,
-    place_row_ref,
-    place_col_ref,
-    route_ref,
-    gain_ref,
-    gate_ref,
-    up_ref,
-    down_ref,
-    out_ref,
-    outbox,
-    full,
-    act,
-    made,
-    returned,
-    total,
-    out_send,
-    out_recv,
-    one_send,
-    one_recv,
-    two_send,
-    two_recv,
-    back_send,
-    back_recv,
-):
-    topk = route_ref.shape[1]
-    rows = mixed_ref.shape[0]
-    capacity, columns = outbox.shape[1:]
-    half = capacity // 2
-    shards = full.shape[1]
-    sp = lax.axis_index("sp")
-    tp = lax.axis_index("tp")
-    beside = tp + 1 - 2 * (tp % 2)
-    across = (tp + 2) % 4
-
-    def partner(number):
-        found, bit = 0, 1
-        while bit < groups:
-            found = found + bit * (((sp // bit) % 2 + (number // bit) % 2) % 2)
-            bit *= 2
-        return found
-
-    def send(src, dst, send_sem, recv_sem, device):
-        return pltpu.make_async_remote_copy(
-            src_ref=src,
-            dst_ref=dst,
-            send_sem=send_sem,
-            recv_sem=recv_sem,
-            device_id=device,
-            device_id_type=pl.DeviceIdType.MESH,
-        )
-
-    def dispatch(i):
-        return send(
-            outbox.at[i], full.at[i, tp], out_send.at[i], out_recv.at[i], (partner(i), tp)
-        )
-
-    def give_back(i):
-        return send(made.at[i], returned.at[i], back_send.at[i], back_recv.at[i], (partner(i), tp))
-
-    def direct(i, held, send_sem, recv_sem, which):
-        device = (sp, beside if which == 0 else across)
-        return send(
-            held.at[i, tp], held.at[i, tp], send_sem.at[i, which], recv_sem.at[i, which], device
-        )
-
-    def relay(i, held, send_sem, recv_sem, which):
-        owner = beside if which == 0 else across
-        device = (sp, across if which == 0 else beside)
-        part = held.at[i, owner, pl.ds(which * half, half)]
-        return send(part, part, send_sem.at[i, 2 + which], recv_sem.at[i, 2 + which], device)
-
-    barrier = pltpu.get_barrier_semaphore()
-    for i in range(1, groups):
-        pl.semaphore_signal(
-            barrier, inc=1, device_id=(partner(i), tp), device_id_type=pl.DeviceIdType.MESH
-        )
-    for other in (beside, across):
-        pl.semaphore_signal(
-            barrier, inc=1, device_id=(sp, other), device_id_type=pl.DeviceIdType.MESH
-        )
-    pl.semaphore_wait(barrier, groups + 1)
-
-    def rows_for(i):
-        numbers = lax.broadcasted_iota(jnp.int32, (capacity, rows), 0) + i * capacity
-        taken = numbers == place_row_ref[0:1, :]
-        for k in range(1, topk):
-            taken = taken | (numbers == place_row_ref[k : k + 1, :])
-        return jnp.dot(
-            jnp.where(taken, 1.0, 0.0).astype(jnp.bfloat16),
-            mixed_ref[...],
-            preferred_element_type=jnp.float32,
-        ).astype(jnp.bfloat16)
-
-    full[0, tp] = rows_for(0)
-
-    def fill(i, carry):
-        outbox[i] = rows_for(i)
-        dispatch(i).start()
-        return carry
-
-    lax.fori_loop(1, groups, fill, 0)
-    total[...] = mixed_ref[...].astype(jnp.float32)
-
-    def start_gather(i, held, send_sem, recv_sem):
-        direct(i, held, send_sem, recv_sem, 0).start()
-        direct(i, held, send_sem, recv_sem, 1).start()
-
-    def pass_on(i, held, send_sem, recv_sem):
-        for which in range(2):
-            direct(i, held, send_sem, recv_sem, which).wait_recv()
-            relay(i, held, send_sem, recv_sem, which).start()
-
-    def finish_gather(i, held, send_sem, recv_sem):
-        for which in range(2):
-            relay(i, held, send_sem, recv_sem, which).wait_recv()
-
-    def hidden(i):
-        square = jnp.zeros((capacity, 1), jnp.float32)
-        for j in range(shards):
-            wide = full[i, j].astype(jnp.float32)
-            square = square + jnp.sum(wide * wide, axis=1, keepdims=True)
-        factor = lax.rsqrt(square / (shards * columns) + NORM_EPS)
-        gate_input = jnp.zeros((capacity, gate_ref.shape[1]), jnp.float32)
-        linear_input = gate_input
-        for j in range(shards):
-            span = slice(j * columns, (j + 1) * columns)
-            gain = gain_ref[0:1, span].astype(jnp.float32)
-            normed = (full[i, j].astype(jnp.float32) * factor * gain).astype(jnp.bfloat16)
-            gate_input = gate_input + jnp.dot(
-                normed, gate_ref[span, :], preferred_element_type=jnp.float32
-            )
-            linear_input = linear_input + jnp.dot(
-                normed, up_ref[span, :], preferred_element_type=jnp.float32
-            )
-        gate_cut = jnp.minimum(gate_input, CLAMP_LIMIT)
-        linear_cut = jnp.clip(linear_input, -CLAMP_LIMIT, CLAMP_LIMIT)
-        act[i, tp] = (gate_cut * jax.nn.sigmoid(SILU_ALPHA * gate_cut) * (linear_cut + 1.0)).astype(
-            jnp.bfloat16
-        )
-
-    def output_rows(i):
-        units = act.shape[3]
-        result = jnp.zeros((capacity, columns), jnp.float32)
-        for j in range(shards):
-            result = result + jnp.dot(
-                act[i, j],
-                down_ref[j * units : (j + 1) * units, :],
-                preferred_element_type=jnp.float32,
-            )
-        return result.astype(jnp.bfloat16)
-
-    def step(i, carry):
-        @pl.when(i < groups)
-        def _():
-            @pl.when(i > 0)
-            def _():
-                dispatch(i).wait_recv()
-
-            start_gather(i, full, one_send, one_recv)
-
-        @pl.when((i >= 1) & (i < groups + 1))
-        def _():
-            pass_on(i - 1, full, one_send, one_recv)
-
-        @pl.when((i >= 2) & (i < groups + 2))
-        def _():
-            finish_gather(i - 2, full, one_send, one_recv)
-            hidden(i - 2)
-            start_gather(i - 2, act, two_send, two_recv)
-
-        @pl.when((i >= 3) & (i < groups + 3))
-        def _():
-            pass_on(i - 3, act, two_send, two_recv)
-
-        @pl.when((i >= 4) & (i < groups + 4))
-        def _():
-            b = i - 4
-            finish_gather(b, act, two_send, two_recv)
-            result = output_rows(b)
-
-            @pl.when(b == 0)
-            def _():
-                returned[0] = result
-
-            @pl.when(b > 0)
-            def _():
-                made[b] = result
-                give_back(b).start()
-
-        @pl.when(i >= 5)
-        def _():
-            b = i - 5
-
-            @pl.when(b > 0)
-            def _():
-                give_back(b).wait_recv()
-
-            numbers = lax.broadcasted_iota(jnp.int32, (rows, capacity), 1) + b * capacity
-            added = total[...]
-            for k in range(topk):
-                taken = jnp.where(numbers == place_col_ref[:, k : k + 1], 1.0, 0.0)
-                picked = jnp.dot(
-                    taken.astype(jnp.bfloat16), returned[b], preferred_element_type=jnp.float32
-                )
-                added = added + route_ref[:, k : k + 1] * picked
-            total[...] = added
-
-        return carry
-
-    lax.fori_loop(0, groups + 5, step, 0)
-    out_ref[...] = total[...].astype(out_ref.dtype)
-
-    def settle(i, carry):
-        @pl.when(i > 0)
-        def _():
-            dispatch(i).wait_send()
-            give_back(i).wait_send()
-
-        for which in range(2):
-            direct(i, full, one_send, one_recv, which).wait_send()
-            relay(i, full, one_send, one_recv, which).wait_send()
-            direct(i, act, two_send, two_recv, which).wait_send()
-            relay(i, act, two_send, two_recv, which).wait_send()
-        return carry
-
-    lax.fori_loop(0, groups, settle, 0)
-
-
-def experts_fused(
-    mixed, place_row, place_col, route_weights, norm_gain, gate_weight, up_weight, down_weight, capacity
-):
-    rows, columns = mixed.shape
-    groups = lax.axis_size("sp")
-    shards = lax.axis_size("tp")
-    units = gate_weight.shape[2]
-    dma = pltpu.SemaphoreType.DMA
-    return pl.pallas_call(
-        functools.partial(experts_kernel, groups),
-        out_shape=jax.ShapeDtypeStruct((rows, columns), jnp.bfloat16),
-        in_specs=[pl.BlockSpec(memory_space=pltpu.VMEM)] * 8,
-        out_specs=pl.BlockSpec(memory_space=pltpu.VMEM),
-        scratch_shapes=[
-            pltpu.VMEM((groups, capacity, columns), jnp.bfloat16),
-            pltpu.VMEM((groups, shards, capacity, columns), jnp.bfloat16),
-            pltpu.VMEM((groups, shards, capacity, units), jnp.bfloat16),
-            pltpu.VMEM((groups, capacity, columns), jnp.bfloat16),
-            pltpu.VMEM((groups, capacity, columns), jnp.bfloat16),
-            pltpu.VMEM((rows, columns), jnp.float32),
-            dma((groups,)),
-            dma((groups,)),
-            dma((groups, 4)),
-            dma((groups, 4)),
-            dma((groups, 4)),
-            dma((groups, 4)),
-            dma((groups,)),
-            dma((groups,)),
-        ],
-        compiler_params=pltpu.CompilerParams(
-            collective_id=1, has_side_effects=True, vmem_limit_bytes=56 * 2**20
-        ),
-    )(
-        mixed,
-        place_row,
-        place_col,
-        route_weights,
-        norm_gain.reshape(1, -1),
-        gate_weight[0],
-        up_weight[0],
-        down_weight[0],
-    )
-
-
-def mix_kernel(
+def half_of(core, tp):
+    return (1 - core) * (tp // 2) + core * (tp % 2)
+
+
+def partner_of(core, tp):
+    return (1 - core) * ((tp + 2) % 4) + core * (tp + 1 - 2 * (tp % 2))
+
+
+def layer_kernel(
     heads,
     groups,
     q_ref,
@@ -402,9 +136,15 @@
     residual_ref,
     index_row_ref,
     index_col_ref,
+    route_ref,
+    gain_ref,
+    gate_ref,
+    up_ref,
+    down_ref,
     out_ref,
     place_row_ref,
     place_col_ref,
+    mixed_ref,
     keys_all,
     values_all,
     gates_all,
@@ -413,12 +153,35 @@
     total,
     summed,
     attended,
+    outbox,
+    full,
+    act,
+    made,
+    returned,
+    blended,
+    gate_all,
+    up_all,
+    down_all,
+    wide_rows,
     next_send,
     next_recv,
     side_send,
     side_recv,
     tp_send,
     tp_recv,
+    weight_send,
+    weight_recv,
+    load_sem,
+    down_send,
+    down_recv,
+    out_send,
+    out_recv,
+    one_send,
+    one_recv,
+    two_send,
+    two_recv,
+    back_send,
+    back_recv,
 ):
     rows, width = q_ref.shape
     head_size = width // heads
@@ -481,16 +244,112 @@
             device_id_type=mesh_id,
         )
 
+    topk = route_ref.shape[1]
+    half, columns = outbox.shape[2:]
+    capacity = 2 * half
+    shards = full.shape[1]
+    mine = half_of(core, tp)
+    pair = partner_of(core, tp)
+    peer = partner_of(1 - core, tp)
+    owners = (tp, pair, peer, (beside + 2) % 4)
+
+    def partner(number):
+        found, bit = 0, 1
+        while bit < groups:
+            found = found + bit * (((sp // bit) % 2 + (number // bit) % 2) % 2)
+            bit *= 2
+        return found
+
+    def send(src, dst, send_sem, recv_sem, device):
+        return pltpu.make_async_remote_copy(
+            src_ref=src,
+            dst_ref=dst,
+            send_sem=send_sem,
+            recv_sem=recv_sem,
+            device_id=device,
+            device_id_type=pl.DeviceIdType.MESH,
+        )
+
+    def dispatch(i, which):
+        group = partner(i)
+        target = tp if which == 0 else partner_of(group % 2, tp)
+        return send(
+            outbox.at[i, which],
+            full.at[i, which],
+            out_send.at[i, which],
+            out_recv.at[i, which],
+            (group, target),
+        )
+
+    def exchange(i, held, send_sem, recv_sem):
+        return send(
+            held.at[i, pl.ds(0, 2)],
+            held.at[i, pl.ds(2, 2)],
+            send_sem.at[i],
+            recv_sem.at[i],
+            (sp, peer),
+        )
+
+    def give_back(i, which):
+        target = tp if which == 0 else pair
+        return send(
+            made.at[i, which],
+            returned.at[i, mine],
+            back_send.at[i, which],
+            back_recv.at[i, mine],
+            (partner(i), target),
+        )
+
+    def arrive_back(i, which):
+        return send(
+            made.at[i, 0],
+            returned.at[i, which],
+            back_send.at[i, 0],
+            back_recv.at[i, which],
+            (sp, pair),
+        )
+
+    loads = []
+    for n, (src, dst) in enumerate(
+        ((gate_ref, gate_all.at[0]), (up_ref, up_all.at[0]), (down_ref, down_all.at[0]))
+    ):
+        loads.append(pltpu.make_async_copy(src, dst, load_sem.at[n]))
+    for load in loads:
+        load.start()
+
     barrier = pltpu.get_barrier_semaphore()
-    for device in (
-        ((sp + 2) % groups, tp),
-        ((sp + groups - 2) % groups, tp),
-        (sibling, tp),
-        (sp, beside),
-        (sp, across),
-    ):
-        pl.semaphore_signal(barrier, inc=1, device_id=device, device_id_type=mesh_id)
-    pl.semaphore_wait(barrier, 5)
+    for i in range(1, groups):
+        pl.semaphore_signal(
+            barrier, inc=1, device_id=(partner(i), tp), device_id_type=pl.DeviceIdType.MESH
+        )
+        pl.semaphore_signal(
+            barrier,
+            inc=1,
+            device_id=(partner(i), partner_of(partner(i) % 2, tp)),
+            device_id_type=pl.DeviceIdType.MESH,
+        )
+        pl.semaphore_signal(
+            barrier, inc=1, device_id=(partner(i), pair), device_id_type=pl.DeviceIdType.MESH
+        )
+    for other in (pair, peer):
+        pl.semaphore_signal(
+            barrier, inc=1, device_id=(sp, other), device_id_type=pl.DeviceIdType.MESH
+        )
+    pl.semaphore_wait(barrier, 3 * groups - 1)
+
+    down_copy = send(down_ref, down_all.at[1], down_send, down_recv, (sp, pair))
+
+    weight_copies = [
+        pltpu.make_async_remote_copy(
+            src_ref=src,
+            dst_ref=dst,
+            send_sem=weight_send.at[n],
+            recv_sem=weight_recv.at[n],
+            device_id=(sp, pair),
+            device_id_type=mesh_id,
+        )
+        for n, (src, dst) in enumerate(((gate_ref, gate_all.at[1]), (up_ref, up_all.at[1])))
+    ]
 
     @pl.when(chip < chips - 1)
     def _():
@@ -502,8 +361,9 @@
         for copy in sideways(sp, True):
             copy.start()
 
-    capacity = 2 * rows * index_row_ref.shape[0] // groups
-    topk = index_row_ref.shape[0]
+    for copy in weight_copies:
+        copy.start()
+
     first = lax.broadcasted_iota(jnp.int32, (rows, rows), 0)
     second = lax.broadcasted_iota(jnp.int32, (rows, rows), 1)
     number = lax.broadcasted_iota(jnp.int32, (rows, 128), 1)
@@ -582,7 +442,7 @@
 
     block(k_ref, v_ref, gates_ref, True)
 
-    def step(d, carry):
+    def ring_step(d, carry):
         mine = sp - 2 * (d // 2)
         other = sibling - 2 * (d // 2)
 
@@ -608,7 +468,7 @@
         block(keys_all.at[now], values_all.at[now], gates_all.at[now], False)
         return carry
 
-    lax.fori_loop(2 - core, 2 * chip + 2, step, 0)
+    lax.fori_loop(2 - core, 2 * chip + 2, ring_step, 0)
 
     for g in range(width // lanes):
         result = jnp.zeros((rows, lanes), jnp.float32)
@@ -621,6 +481,7 @@
         attended[tp, :, g * lanes : (g + 1) * lanes] = result.astype(jnp.bfloat16)
     direct(0).start()
     direct(1).start()
+    down_copy.start()
 
     def projected(owner):
         return jnp.dot(
@@ -636,7 +497,153 @@
         mixed = mixed + projected(owner)
     relay(0).wait_recv()
     relay(1).wait_recv()
-    out_ref[...] = (mixed + projected((beside + 2) % 4)).astype(out_ref.dtype)
+    mixed_ref[...] = (mixed + projected((beside + 2) % 4)).astype(mixed_ref.dtype)
+
+    def rows_for(i):
+        flip = half_of(partner(i) % 2, tp)
+        place = lax.broadcasted_iota(jnp.int32, (capacity, rows), 0) + flip * half
+        numbers = jnp.where(place >= capacity, place - capacity, place) + i * capacity
+        taken = numbers == place_row_ref[0:1, :]
+        for k in range(1, topk):
+            taken = taken | (numbers == place_row_ref[k : k + 1, :])
+        return jnp.dot(
+            jnp.where(taken, 1.0, 0.0).astype(jnp.bfloat16),
+            mixed_ref[...],
+            preferred_element_type=jnp.float32,
+        ).astype(jnp.bfloat16)
+
+    first = rows_for(0)
+    full[0, 0] = first[:half]
+    outbox[0, 1] = first[half:]
+    dispatch(0, 1).start()
+
+    def fill(i, carry):
+        made_rows = rows_for(i)
+        outbox[i, 0] = made_rows[:half]
+        outbox[i, 1] = made_rows[half:]
+        dispatch(i, 0).start()
+        dispatch(i, 1).start()
+        return carry
+
+    lax.fori_loop(1, groups, fill, 0)
+    blended[...] = mixed_ref[...].astype(jnp.float32)
+    for load in loads:
+        load.wait()
+    for copy in weight_copies:
+        copy.wait_recv()
+
+    def hidden(i):
+        square = jnp.zeros((half, 1), jnp.float32)
+        for j in range(shards):
+            wide = full[i, j].astype(jnp.float32)
+            square = square + jnp.sum(wide * wide, axis=1, keepdims=True)
+        factor = lax.rsqrt(square / (shards * columns) + NORM_EPS)
+        for j in range(shards):
+            span = pl.ds(pl.multiple_of(owners[j] * columns, columns), columns)
+            gain = gain_ref[0:1, span].astype(jnp.float32)
+            wide_rows[:, span] = (full[i, j].astype(jnp.float32) * factor * gain).astype(
+                jnp.bfloat16
+            )
+        for c in range(2):
+            gate_input = jnp.dot(
+                wide_rows[...], gate_all[c], preferred_element_type=jnp.float32
+            )
+            linear_input = jnp.dot(wide_rows[...], up_all[c], preferred_element_type=jnp.float32)
+            gate_cut = jnp.minimum(gate_input, CLAMP_LIMIT)
+            linear_cut = jnp.clip(linear_input, -CLAMP_LIMIT, CLAMP_LIMIT)
+            act[i, c] = (
+                gate_cut * jax.nn.sigmoid(SILU_ALPHA * gate_cut) * (linear_cut + 1.0)
+            ).astype(jnp.bfloat16)
+
+    def output_rows(i, c):
+        return jnp.dot(
+            wide_rows[...], down_all[c], preferred_element_type=jnp.float32
+        ).astype(jnp.bfloat16)
+
+    def step(i, carry):
+        @pl.when(i < groups)
+        def _():
+            @pl.when(i > 0)
+            def _():
+                dispatch(i, 0).wait_recv()
+
+            dispatch(i, 1).wait_recv()
+            exchange(i, full, one_send, one_recv).start()
+
+        @pl.when((i >= 1) & (i < groups + 1))
+        def _():
+            exchange(i - 1, full, one_send, one_recv).wait_recv()
+            hidden(i - 1)
+            exchange(i - 1, act, two_send, two_recv).start()
+
+        @pl.when((i >= 2) & (i < groups + 2))
+        def _():
+            b = i - 2
+
+            @pl.when(b == 0)
+            def _():
+                down_copy.wait_recv()
+
+            exchange(b, act, two_send, two_recv).wait_recv()
+            for j in range(shards):
+                span = pl.ds(pl.multiple_of(owners[j] * columns, columns), columns)
+                wide_rows[:, span] = act[b, j]
+            made[b, 1] = output_rows(b, 1)
+            give_back(b, 1).start()
+            result = output_rows(b, 0)
+
+            @pl.when(b == 0)
+            def _():
+                returned[0, mine] = result
+
+            @pl.when(b > 0)
+            def _():
+                made[b, 0] = result
+                give_back(b, 0).start()
+
+        @pl.when(i >= 3)
+        def _():
+            b = i - 3
+
+            @pl.when(b == 0)
+            def _():
+                arrive_back(0, 1 - mine).wait_recv()
+
+            @pl.when(b > 0)
+            def _():
+                arrive_back(b, 0).wait_recv()
+                arrive_back(b, 1).wait_recv()
+
+            numbers = lax.broadcasted_iota(jnp.int32, (rows, capacity), 1) + b * capacity
+            added = blended[...]
+            rows_back = returned[b].reshape(capacity, columns)
+            for k in range(topk):
+                taken = jnp.where(numbers == place_col_ref[:, k : k + 1], 1.0, 0.0)
+                picked = jnp.dot(
+                    taken.astype(jnp.bfloat16), rows_back, preferred_element_type=jnp.float32
+                )
+                added = added + route_ref[:, k : k + 1] * picked
+            blended[...] = added
+
+        return carry
+
+    lax.fori_loop(0, groups + 3, step, 0)
+    out_ref[...] = blended[...].astype(out_ref.dtype)
+
+    def settle(i, carry):
+        @pl.when(i > 0)
+        def _():
+            dispatch(i, 0).wait_send()
+            give_back(i, 0).wait_send()
+
+        dispatch(i, 1).wait_send()
+        give_back(i, 1).wait_send()
+        exchange(i, full, one_send, one_recv).wait_send()
+        exchange(i, act, two_send, two_recv).wait_send()
+        return carry
+
+    lax.fori_loop(0, groups, settle, 0)
+    down_copy.wait_send()
 
     for which in range(2):
         direct(which).wait_send()
@@ -652,7 +659,7 @@
         for copy in sideways(sp, True):
             copy.wait_send()
 
-    def settle(d, carry):
+    def settle_ring(d, carry):
         @pl.when(chip < chips - 1)
         def _():
             for copy in onward(sp - 2 * d):
@@ -662,25 +669,45 @@
             copy.wait_send()
         return carry
 
-    lax.fori_loop(1, chip + 1, settle, 0)
-
-
-def mix_fused(query_rows, key_rows, value_rows, gates, output_weight, residual, index):
+    lax.fori_loop(1, chip + 1, settle_ring, 0)
+    for copy in weight_copies:
+        copy.wait_send()
+
+
+def layer_fused(
+    query_rows,
+    key_rows,
+    value_rows,
+    gates,
+    output_weight,
+    residual,
+    index,
+    route_weights,
+    norm_gain,
+    gate_weight,
+    up_weight,
+    down_weight,
+    capacity,
+):
     rows, width = query_rows.shape
+    columns = residual.shape[1]
     heads = gates.shape[0]
     groups = lax.axis_size("sp")
+    shards = lax.axis_size("tp")
     lanes = min(width, 128)
+    depth, units = gate_weight.shape
+    half = capacity // 2
     dma = pltpu.SemaphoreType.DMA
     return pl.pallas_call(
-        functools.partial(mix_kernel, heads, groups),
-        out_shape=(
-            jax.ShapeDtypeStruct(residual.shape, jnp.bfloat16),
-            jax.ShapeDtypeStruct(index.shape[::-1], jnp.int32),
-            jax.ShapeDtypeStruct(index.shape, jnp.int32),
-        ),
-        in_specs=[pl.BlockSpec(memory_space=pltpu.VMEM)] * 8,
-        out_specs=(pl.BlockSpec(memory_space=pltpu.VMEM),) * 3,
+        functools.partial(layer_kernel, heads, groups),
+        out_shape=jax.ShapeDtypeStruct(residual.shape, jnp.bfloat16),
+        in_specs=[pl.BlockSpec(memory_space=pltpu.VMEM)] * 10
+        + [pl.BlockSpec(memory_space=pl.ANY)] * 3,
+        out_specs=pl.BlockSpec(memory_space=pltpu.VMEM),
         scratch_shapes=[
+            pltpu.VMEM(index.shape[::-1], jnp.int32),
+            pltpu.VMEM(index.shape, jnp.int32),
+            pltpu.VMEM((rows, columns), jnp.bfloat16),
             pltpu.VMEM((groups, rows, width), jnp.bfloat16),
             pltpu.VMEM((groups, rows, width), jnp.bfloat16),
             pltpu.VMEM((groups, heads, rows), jnp.float32),
@@ -689,17 +716,54 @@
             pltpu.VMEM((heads, rows, 128), jnp.float32),
             pltpu.VMEM((heads, rows, lanes), jnp.float32),
             pltpu.VMEM((4, rows, width), jnp.bfloat16),
+            pltpu.VMEM((groups, 2, half, columns), jnp.bfloat16),
+            pltpu.VMEM((groups, shards, half, columns), jnp.bfloat16),
+            pltpu.VMEM((groups, shards, half, units), jnp.bfloat16),
+            pltpu.VMEM((groups, 2, half, columns), jnp.bfloat16),
+            pltpu.VMEM((groups, 2, half, columns), jnp.bfloat16),
+            pltpu.VMEM((rows, columns), jnp.float32),
+            pltpu.VMEM((2, depth, units), jnp.bfloat16),
+            pltpu.VMEM((2, depth, units), jnp.bfloat16),
+            pltpu.VMEM((2, shards * units, columns), jnp.bfloat16),
+            pltpu.VMEM((half, shards * columns), jnp.bfloat16),
             dma((groups, 3)),
             dma((groups, 3)),
             dma((groups, 3)),
             dma((groups, 3)),
             dma((4,)),
             dma((4,)),
+            dma((2,)),
+            dma((2,)),
+            dma((3,)),
+            dma(()),
+            dma(()),
+            dma((groups, 2)),
+            dma((groups, 2)),
+            dma((groups,)),
+            dma((groups,)),
+            dma((groups,)),
+            dma((groups,)),
+            dma((groups, 2)),
+            dma((groups, 2)),
         ],
         compiler_params=pltpu.CompilerParams(
-            collective_id=2, has_side_effects=True, vmem_limit_bytes=40 * 2**20
+            collective_id=1, has_side_effects=True, vmem_limit_bytes=60 * 2**20
         ),
-    )(query_rows, key_rows, value_rows, gates, output_weight, residual, index.T, index)
+    )(
+        query_rows,
+        key_rows,
+        value_rows,
+        gates,
+        output_weight,
+        residual,
+        index.T,
+        index,
+        route_weights,
+        norm_gain.reshape(1, -1),
+        gate_weight,
+        up_weight,
+        down_weight,
+    )
 
 
 def body(
@@ -726,18 +790,19 @@
 
     if lax.axis_size("tp") == 4 and local_experts == 1 and groups in (4, 8):
         index = expert_index ^ lax.axis_index("sp")
-        mixed, place_row, place_col = mix_fused(
-            query_rows, key_rows, value_rows, cum_gates.T, output_weight, residual, index
-        )
-        return experts_fused(
-            mixed,
-            place_row,
-            place_col,
+        return layer_fused(
+            query_rows,
+            key_rows,
+            value_rows,
+            cum_gates.T,
+            output_weight,
+            residual,
+            index,
             route_weights,
             norm_gain,
-            gate_weight,
-            up_weight,
-            down_weight,
+            gate_weight[0],
+            up_weight[0],
+            down_weight[0],
             capacity,
         )
 

time: 243 us -> 192 us (0.79)
  Pallas kernels: 231 us -> 184 us
  local copies, waits for them, and re-layouts: 11.4 us -> 6.21 us
    pallas_call x2 -> x1, Pallas kernels: 231 us -> 184 us  [layer_fused(): pl.pallas_call(functools.partial(layer_kernel, heads, groups), out_shape=...]
    unnamed x21 -> x3, local copies, waits for them, and re-layouts: 9.86 us -> 4.23 us
where the time goes in v1:
time: 192 us; the launch traced here: 191 us
  Pallas kernels  184 us (96%)
  local copies, waits for them, and re-layouts  6.21 us (3%)
    pallas_call x1, Pallas kernels, layer_fused(): pl.pallas_call(functools.partial(layer_kernel, heads, groups), out_shape=...  184 us
    unnamed x3, local copies, waits for them, and re-layouts  4.23 us

profile of v1, /device:TPU:17, one launch (start us, length us, event | category | flops | bytes accessed | tf_op | source)
XLA Modules:
  0.0 191.3 jit_solution(17268215157639843534)
XLA Ops:
  0.0 1.3 reshape.3.gain_ref
  1.3 0.8 copy.13
  2.1 0.7 copy.14.index_row_ref
  2.8 0.7 broadcast_xor_fusion.index_col_ref
  3.6 1.5 copy.15.route_ref
  5.1 184.4 %shard_map.118 = bf16[512,512]{1,0:T(8,128)(2,1)} custom-call(bf16[512,256]{1,0:T(8,128)(2,1)} %q_ref.1, bf16[512,256]{1,0:T(8,128)(2,1)} %k_ref.1, bf16[512,256]{1,0:T(8,128)(2,1)} %v_ref.1, f32[4,512]{1,0:T(4,128)} %bitcast.9, bf16[1024,512]{1,0:T(8,128)(2,1)} %weight_ref.1, bf16[512,512]{1,0:T(8,128)(2,1)} %residual_ref.1, s32[2,512]{1,0:T(2,128)} %copy.14.index_row_ref, ...), custom_call_target="tpu_custom_call" | custom-call | tf_op jit(solution)/shard_map/pallas_call | solution.py:701
  189.5 1.9 copy.17
  (1 shorter events, 0.0 us)

commit v2 on v1

--- a/solution.py
+++ b/solution.py
@@ -145,9 +145,14 @@
     place_row_ref,
     place_col_ref,
     mixed_ref,
-    keys_all,
-    values_all,
+    kv_out,
+    q_out,
+    kv_all,
+    q_all,
     gates_all,
+    gate_pair,
+    packed,
+    heads_in,
     masked_q,
     top,
     total,
@@ -163,10 +168,13 @@
     up_all,
     down_all,
     wide_rows,
-    next_send,
-    next_recv,
+    kv_send,
     side_send,
-    side_recv,
+    kv_recv,
+    q_send,
+    q_recv,
+    head_send,
+    head_recv,
     tp_send,
     tp_recv,
     weight_send,
@@ -198,29 +206,7 @@
     across = (tp + 2) % 4
     mesh_id = pl.DeviceIdType.MESH
     scale = head_size ** (-0.5)
-
-    def copies(number, own, device, send_sem, recv_sem):
-        made = []
-        for n, (mine, held) in enumerate(
-            ((k_ref, keys_all), (v_ref, values_all), (gates_ref, gates_all))
-        ):
-            made.append(
-                pltpu.make_async_remote_copy(
-                    src_ref=mine if own else held.at[number],
-                    dst_ref=held.at[number],
-                    send_sem=send_sem.at[number, n],
-                    recv_sem=recv_sem.at[number, n],
-                    device_id=device,
-                    device_id_type=mesh_id,
-                )
-            )
-        return made
-
-    def onward(number, own=False):
-        return copies(number, own, ((sp + 2) % groups, tp), next_send, next_recv)
-
-    def sideways(number, own=False):
-        return copies(number, own, (sibling, tp), side_send, side_recv)
+    lead = (sp + chip) % 2
 
     def direct(which):
         return pltpu.make_async_remote_copy(
@@ -270,6 +256,42 @@
             device_id_type=pl.DeviceIdType.MESH,
         )
 
+    def spread(head):
+        device = (2 * head + core, tp)
+        return [
+            send(src, dst.at[sp], kv_send.at[head, n], kv_recv.at[sp, n], device)
+            for n, (src, dst) in enumerate(((kv_out.at[head], kv_all), (gates_ref, gates_all)))
+        ]
+
+    def sideways(number, own=False):
+        return [
+            send(src, dst.at[number], side_send.at[number, n], kv_recv.at[number, n], (sibling, tp))
+            for n, (src, dst) in enumerate(
+                (
+                    (kv_all.at[number], kv_all),
+                    (gates_ref if own else gates_all.at[number], gates_all),
+                )
+            )
+        ]
+
+    def ask(head):
+        return send(
+            q_out.at[head],
+            q_all.at[chip],
+            q_send.at[head],
+            q_recv.at[chip],
+            (2 * head + lead, tp),
+        )
+
+    def answer(slot):
+        return send(
+            packed.at[slot],
+            heads_in.at[chip],
+            head_send.at[slot],
+            head_recv.at[chip],
+            (2 * slot + (slot + core) % 2, tp),
+        )
+
     def dispatch(i, which):
         group = partner(i)
         target = tp if which == 0 else partner_of(group % 2, tp)
@@ -351,16 +373,44 @@
         for n, (src, dst) in enumerate(((gate_ref, gate_all.at[1]), (up_ref, up_all.at[1])))
     ]
 
-    @pl.when(chip < chips - 1)
+    lane = lax.broadcasted_iota(jnp.int32, (rows, lanes), 1)
+    low = lane < head_size
+    short = rows // 2
+    short_low = low[:short]
+
+    def turned(wide):
+        return pltpu.roll(wide, head_size, 1)
+
+    for g in range(width // lanes):
+        part = slice(g * lanes, (g + 1) * lanes)
+        wide = q_ref[:, part].astype(jnp.float32) * scale
+        tail = turned(wide[short:])
+        q_out[2 * g] = jnp.where(short_low, wide[:short], tail).astype(jnp.bfloat16)
+        q_out[2 * g + 1] = jnp.where(short_low, tail, wide[:short]).astype(jnp.bfloat16)
+    for s in range(1, chips):
+        ask(partner(2 * s) // 2).start()
+
+    @pl.when(lead != core)
     def _():
-        for copy in onward(sp, True):
+        ask(chip).start()
+
+    @pl.when(lead == core)
+    def _():
+        q_all[chip] = q_out[chip]
+
+    for g in range(width // lanes):
+        part = slice(g * lanes, (g + 1) * lanes)
+        keys = k_ref[:, part].astype(jnp.float32)
+        values = turned(v_ref[:, part].astype(jnp.float32))
+        kv_out[2 * g] = jnp.where(low, keys, values).astype(jnp.bfloat16)
+        kv_out[2 * g + 1] = jnp.where(low, values, keys).astype(jnp.bfloat16)
+    for s in range(1, chips):
+        for copy in spread(partner(2 * s) // 2):
             copy.start()
-
-    @pl.when(core == 0)
-    def _():
-        for copy in sideways(sp, True):
-            copy.start()
-
+    kv_all[sp] = kv_out[chip]
+    gates_all[sp] = gates_ref[...]
+    for copy in sideways(sp, True):
+        copy.start()
     for copy in weight_copies:
         copy.start()
 
@@ -393,92 +443,120 @@
         rank = jnp.sum(jnp.where(number == expert, before, 0.0), axis=0, keepdims=True)
         place_row_ref[k : k + 1, :] = expert * capacity + rank.astype(jnp.int32)
 
-    lane = lax.broadcasted_iota(jnp.int32, (rows, lanes), 1)
-    for h in range(heads):
-        group, inside = divmod(h * head_size, lanes)
-        part = q_ref[:, group * lanes : (group + 1) * lanes].astype(jnp.float32) * scale
-        keep = (lane >= inside) & (lane < inside + head_size)
-        masked_q[h] = jnp.where(keep, part, 0.0).astype(jnp.bfloat16)
+    odd = chip % 2
+    key_lane = (lane // head_size) == odd
+    short_key = key_lane[:short]
     top[...] = jnp.full(top.shape, -1e30, jnp.float32)
     total[...] = jnp.zeros(total.shape, jnp.float32)
     summed[...] = jnp.zeros(summed.shape, jnp.float32)
-
-    def block(key_block, value_block, gate_block, diagonal):
-        for h in range(heads):
-            group = h * head_size // lanes
-            keys = key_block[:, group * lanes : (group + 1) * lanes]
-            values = value_block[:, group * lanes : (group + 1) * lanes]
-            gates = gate_block[h : h + 1, :]
-            for t in range(tiles):
-                span = slice(t * tile, (t + 1) * tile)
-                count = (t + 1) * tile if diagonal else rows
-                scores = lax.dot_general(
-                    masked_q[h, span],
-                    keys[:count],
-                    (((1,), (1,)), ((), ())),
-                    preferred_element_type=jnp.float32,
-                )
-                scores = scores - gates[:, :count]
-                if diagonal:
-                    row = lax.broadcasted_iota(jnp.int32, (tile, count), 0) + t * tile
-                    col = lax.broadcasted_iota(jnp.int32, (tile, count), 1)
-                    scores = jnp.where(col <= row, scores, -jnp.inf)
-                old = top[h, span]
-                new = jnp.maximum(old, jnp.max(scores, axis=1, keepdims=True))
-                raised = jnp.exp(scores - new[:, :1])
-                shrink = jnp.exp(old - new)
-                part = raised[:, :128]
-                for c in range(128, count, 128):
-                    part = part + raised[:, c : c + 128]
-                top[h, span] = new
-                total[h, span] = total[h, span] * shrink + part
-                product = lax.dot_general(
-                    raised.astype(jnp.bfloat16),
-                    values[:count],
-                    (((1,), (0,)), ((), ())),
-                    preferred_element_type=jnp.float32,
-                )
-                summed[h, span] = summed[h, span] * shrink[:, :lanes] + product
-
-    block(k_ref, v_ref, gates_ref, True)
-
-    def ring_step(d, carry):
-        mine = sp - 2 * (d // 2)
-        other = sibling - 2 * (d // 2)
-
-        @pl.when((d % 2 == 0) & (d >= 2))
-        def _():
-            for copy in onward(mine):
+    for n in range(chips):
+
+        @pl.when((n != chip) | (lead != core))
+        def _():
+            send(
+                q_out.at[0], q_all.at[n], q_send.at[0], q_recv.at[n], (sibling, tp)
+            ).wait_recv()
+
+        part = q_all[n].astype(jnp.float32)
+        masked_q[n, :short] = jnp.where(short_key, part, 0.0).astype(jnp.bfloat16)
+        masked_q[n, short:] = jnp.where(short_key, turned(part), 0.0).astype(jnp.bfloat16)
+
+    def block(slot, number, offset):
+        span_keys = 2 * rows
+        for t in range(tiles):
+            span = slice(t * tile, (t + 1) * tile)
+            count = span_keys if offset is None else offset + (t + 1) * tile
+            pair_kv = kv_all[pl.ds(2 * number, 2)].reshape(span_keys, lanes)[:count]
+            scores = lax.dot_general(
+                masked_q[slot, span],
+                pair_kv,
+                (((1,), (1,)), ((), ())),
+                preferred_element_type=jnp.float32,
+            )
+            scores = scores - gate_pair[0:1, :count]
+            if offset is not None:
+                row = lax.broadcasted_iota(jnp.int32, (tile, count), 0) + t * tile + offset
+                col = lax.broadcasted_iota(jnp.int32, (tile, count), 1)
+                scores = jnp.where(col <= row, scores, -jnp.inf)
+            old = top[slot, span]
+            new = jnp.maximum(old, jnp.max(scores, axis=1, keepdims=True))
+            raised = jnp.exp(scores - new[:, :1])
+            shrink = jnp.exp(old - new)
+            part = raised[:, :128]
+            for c in range(128, count, 128):
+                part = part + raised[:, c : c + 128]
+            top[slot, span] = new
+            total[slot, span] = total[slot, span] * shrink + part
+            product = lax.dot_general(
+                raised.astype(jnp.bfloat16),
+                pair_kv,
+                (((1,), (0,)), ((), ())),
+                preferred_element_type=jnp.float32,
+            )
+            summed[slot, span] = summed[slot, span] * shrink[:, :lanes] + product
+
+    def chip_step(s, carry):
+        number = partner(2 * s) // 2
+        near = 2 * number + core
+
+        @pl.when(s > 0)
+        def _():
+            for copy in sideways(near):
                 copy.wait_recv()
-
-            @pl.when(chip < chips - 1)
-            def _():
-                for copy in onward(mine):
-                    copy.start()
-
-            for copy in sideways(mine):
+            for copy in sideways(near):
                 copy.start()
 
-        @pl.when(d % 2 == 1)
-        def _():
-            for copy in sideways(other):
-                copy.wait_recv()
-
-        now = mine * (1 - d % 2) + other * (d % 2)
-        block(keys_all.at[now], values_all.at[now], gates_all.at[now], False)
+        for copy in sideways(2 * number + 1 - core):
+            copy.wait_recv()
+        gate_pair[0:1, :rows] = gates_all[2 * number, pl.ds(chip, 1), :]
+        gate_pair[0:1, rows:] = gates_all[2 * number + 1, pl.ds(chip, 1), :]
+
+        @pl.when((number + core) % 2 == 0)
+        def _():
+            block(number, number, 0)
+
+        @pl.when((number + core) % 2 == 1)
+        def _():
+            block(number, number, rows)
+
+        def full_step(slot, inner):
+            block(slot, number, None)
+            return inner
+
+        lax.fori_loop(number + 1, chips, full_step, 0)
         return carry
 
-    lax.fori_loop(2 - core, 2 * chip + 2, ring_step, 0)
+    lax.fori_loop(0, chips, chip_step, 0)
+
+    for n in range(chips):
+        result = summed[n] / jnp.sum(total[n], axis=1, keepdims=True)
+        folded = jnp.where(short_key, turned(result[short:]), result[:short])
+        packed[n] = folded.astype(jnp.bfloat16)
+
+        @pl.when((n != chip) | (lead != core))
+        def _():
+            answer(n).start()
+
+        @pl.when((n == chip) & (lead == core))
+        def _():
+            heads_in[chip] = packed[n]
+
+    for n in range(chips):
+
+        @pl.when((n != chip) | (lead != core))
+        def _():
+            send(
+                packed.at[0], heads_in.at[n], head_send.at[0], head_recv.at[n], (sibling, tp)
+            ).wait_recv()
 
     for g in range(width // lanes):
-        result = jnp.zeros((rows, lanes), jnp.float32)
-        for h in range(heads):
-            if h * head_size // lanes == g:
-                inside = h * head_size % lanes
-                keep = (lane >= inside) & (lane < inside + head_size)
-                whole = jnp.sum(total[h], axis=1, keepdims=True)
-                result = jnp.where(keep, summed[h] / whole, result)
-        attended[tp, :, g * lanes : (g + 1) * lanes] = result.astype(jnp.bfloat16)
+        even = heads_in[2 * g].astype(jnp.float32)
+        uneven = heads_in[2 * g + 1].astype(jnp.float32)
+        part = slice(g * lanes, (g + 1) * lanes)
+        attended[tp, :short, part] = jnp.where(short_low, turned(even), turned(uneven)).astype(
+            jnp.bfloat16
+        )
+        attended[tp, short:, part] = jnp.where(short_low, even, uneven).astype(jnp.bfloat16)
     direct(0).start()
     direct(1).start()
     down_copy.start()
@@ -649,27 +727,25 @@
         direct(which).wait_send()
         relay(which).wait_send()
 
-    @pl.when(chip < chips - 1)
+    for s in range(1, chips):
+        ask(partner(2 * s) // 2).wait_send()
+        for copy in spread(partner(2 * s) // 2):
+            copy.wait_send()
+        for copy in sideways(2 * (partner(2 * s) // 2) + core):
+            copy.wait_send()
+    for copy in sideways(sp, True):
+        copy.wait_send()
+
+    @pl.when(lead != core)
     def _():
-        for copy in onward(sp, True):
-            copy.wait_send()
-
-    @pl.when(core == 0)
-    def _():
-        for copy in sideways(sp, True):
-            copy.wait_send()
-
-    def settle_ring(d, carry):
-        @pl.when(chip < chips - 1)
-        def _():
-            for copy in onward(sp - 2 * d):
-                copy.wait_send()
-
-        for copy in sideways(sp - 2 * d):
-            copy.wait_send()
-        return carry
-
-    lax.fori_loop(1, chip + 1, settle_ring, 0)
+        ask(chip).wait_send()
+
+    for n in range(chips):
+
+        @pl.when((n != chip) | (lead != core))
+        def _():
+            answer(n).wait_send()
+
     for copy in weight_copies:
         copy.wait_send()
 
@@ -708,9 +784,14 @@
             pltpu.VMEM(index.shape[::-1], jnp.int32),
             pltpu.VMEM(index.shape, jnp.int32),
             pltpu.VMEM((rows, columns), jnp.bfloat16),
-            pltpu.VMEM((groups, rows, width), jnp.bfloat16),
-            pltpu.VMEM((groups, rows, width), jnp.bfloat16),
+            pltpu.VMEM((heads, rows, lanes), jnp.bfloat16),
+            pltpu.VMEM((heads, rows // 2, lanes), jnp.bfloat16),
+            pltpu.VMEM((groups, rows, lanes), jnp.bfloat16),
+            pltpu.VMEM((heads, rows // 2, lanes), jnp.bfloat16),
             pltpu.VMEM((groups, heads, rows), jnp.float32),
+            pltpu.VMEM((8, 2 * rows), jnp.float32),
+            pltpu.VMEM((heads, rows // 2, lanes), jnp.bfloat16),
+            pltpu.VMEM((heads, rows // 2, lanes), jnp.bfloat16),
             pltpu.VMEM((heads, rows, lanes), jnp.bfloat16),
             pltpu.VMEM((heads, rows, 128), jnp.float32),
             pltpu.VMEM((heads, rows, 128), jnp.float32),
@@ -726,10 +807,13 @@
             pltpu.VMEM((2, depth, units), jnp.bfloat16),
             pltpu.VMEM((2, shards * units, columns), jnp.bfloat16),
             pltpu.VMEM((half, shards * columns), jnp.bfloat16),
-            dma((groups, 3)),
-            dma((groups, 3)),
-            dma((groups, 3)),
-            dma((groups, 3)),
+            dma((heads, 2)),
+            dma((groups, 2)),
+            dma((groups, 2)),
+            dma((heads,)),
+            dma((heads,)),
+            dma((heads,)),
+            dma((heads,)),
             dma((4,)),
             dma((4,)),
             dma((2,)),
@@ -788,7 +872,13 @@
     capacity = 2 * rows * topk // experts
     heads = cum_gates.shape[1]
 
-    if lax.axis_size("tp") == 4 and local_experts == 1 and groups in (4, 8):
+    if (
+        lax.axis_size("tp") == 4
+        and local_experts == 1
+        and groups == 8
+        and heads == 4
+        and query_rows.shape[1] == heads * 64
+    ):
         index = expert_index ^ lax.axis_index("sp")
         return layer_fused(
             query_rows,

time: 192 us -> 192 us (level)
  no operation moved by 1% of the time
where the time goes in v2:
time: 192 us
  Pallas kernels  185 us (96%)
  local copies, waits for them, and re-layouts  6.21 us (3%)
    pallas_call x1, Pallas kernels, layer_fused(): pl.pallas_call(functools.partial(layer_kernel, heads, groups), out_shape=...  185 us
    unnamed x3, local copies, waits for them, and re-layouts  4.23 us

profile of v2, /device:TPU:17, one launch (start us, length us, event | category | flops | bytes accessed | tf_op | source)
XLA Modules:
  0.0 192.1 jit_solution(17242413961830765999)
XLA Ops:
  0.0 1.3 reshape.3.gain_ref
  1.3 0.8 copy.13
  2.1 0.7 copy.14.index_row_ref
  2.8 0.7 broadcast_xor_fusion.index_col_ref
  3.6 1.5 copy.15.route_ref
  5.1 185.1 %shard_map.118 = bf16[512,512]{1,0:T(8,128)(2,1)} custom-call(bf16[512,256]{1,0:T(8,128)(2,1)} %q_ref.1, bf16[512,256]{1,0:T(8,128)(2,1)} %k_ref.1, bf16[512,256]{1,0:T(8,128)(2,1)} %v_ref.1, f32[4,512]{1,0:T(4,128)} %bitcast.9, bf16[1024,512]{1,0:T(8,128)(2,1)} %weight_ref.1, bf16[512,512]{1,0:T(8,128)(2,1)} %residual_ref.1, s32[2,512]{1,0:T(2,128)} %copy.14.index_row_ref, ...), custom_call_target="tpu_custom_call" | custom-call | tf_op jit(solution)/shard_map/pallas_call | solution.py:777
  190.3 1.9 copy.17
  (1 shorter events, 0.0 us)

commit v3 on v2

--- a/solution.py
+++ b/solution.py
@@ -134,8 +134,7 @@
     gates_ref,
     weight_ref,
     residual_ref,
-    index_row_ref,
-    index_col_ref,
+    index_ref,
     route_ref,
     gain_ref,
     gate_ref,
@@ -143,7 +142,9 @@
     down_ref,
     out_ref,
     place_row_ref,
-    place_col_ref,
+    facts,
+    facts_col,
+    gain_row,
     mixed_ref,
     kv_out,
     q_out,
@@ -230,7 +231,7 @@
             device_id_type=mesh_id,
         )
 
-    topk = route_ref.shape[1]
+    topk = route_ref.shape[0]
     half, columns = outbox.shape[2:]
     capacity = 2 * half
     shards = full.shape[1]
@@ -360,18 +361,29 @@
     pl.semaphore_wait(barrier, 3 * groups - 1)
 
     down_copy = send(down_ref, down_all.at[1], down_send, down_recv, (sp, pair))
-
-    weight_copies = [
-        pltpu.make_async_remote_copy(
-            src_ref=src,
-            dst_ref=dst,
-            send_sem=weight_send.at[n],
-            recv_sem=weight_recv.at[n],
-            device_id=(sp, pair),
-            device_id_type=mesh_id,
-        )
-        for n, (src, dst) in enumerate(((gate_ref, gate_all.at[1]), (up_ref, up_all.at[1])))
-    ]
+    pieces = weight_send.shape[0]
+    depth = gate_ref.shape[0] // pieces
+
+    def weight_copies(number):
+        part = pl.ds(pl.multiple_of(number * depth, depth), depth)
+        return [
+            send(
+                src.at[part],
+                dst.at[1, part],
+                weight_send.at[number, n],
+                weight_recv.at[number, n],
+                (sp, pair),
+            )
+            for n, (src, dst) in enumerate(((gate_ref, gate_all), (up_ref, up_all)))
+        ]
+
+    def push(number):
+        for copy in weight_copies(number):
+            copy.start()
+
+    early = pieces - 1 - chips
+    for number in range(early):
+        push(number)
 
     lane = lax.broadcasted_iota(jnp.int32, (rows, lanes), 1)
     low = lane < head_size
@@ -411,37 +423,27 @@
     gates_all[sp] = gates_ref[...]
     for copy in sideways(sp, True):
         copy.start()
-    for copy in weight_copies:
-        copy.start()
 
     first = lax.broadcasted_iota(jnp.int32, (rows, rows), 0)
     second = lax.broadcasted_iota(jnp.int32, (rows, rows), 1)
-    number = lax.broadcasted_iota(jnp.int32, (rows, 128), 1)
-    named = jnp.zeros((rows, 128), jnp.float32)
-    for k in range(topk):
-        named = named + jnp.where(number == index_col_ref[:, k : k + 1], 1.0, 0.0)
-    before = jnp.dot(
-        jnp.where(second < first, 1.0, 0.0).astype(jnp.bfloat16),
-        named.astype(jnp.bfloat16),
-        preferred_element_type=jnp.float32,
-    )
-    for k in range(topk):
-        expert = index_col_ref[:, k : k + 1]
-        rank = jnp.sum(jnp.where(number == expert, before, 0.0), axis=1, keepdims=True)
-        place_col_ref[:, k : k + 1] = expert * capacity + rank.astype(jnp.int32)
     number = lax.broadcasted_iota(jnp.int32, (128, rows), 0)
+    chosen = [index_ref[k : k + 1, :] ^ sp for k in range(topk)]
     named = jnp.zeros((128, rows), jnp.float32)
     for k in range(topk):
-        named = named + jnp.where(number == index_row_ref[k : k + 1, :], 1.0, 0.0)
+        named = named + jnp.where(number == chosen[k], 1.0, 0.0)
     before = jnp.dot(
         named.astype(jnp.bfloat16),
         jnp.where(first < second, 1.0, 0.0).astype(jnp.bfloat16),
         preferred_element_type=jnp.float32,
     )
+    facts[...] = jnp.zeros(facts.shape, jnp.float32)
     for k in range(topk):
-        expert = index_row_ref[k : k + 1, :]
-        rank = jnp.sum(jnp.where(number == expert, before, 0.0), axis=0, keepdims=True)
-        place_row_ref[k : k + 1, :] = expert * capacity + rank.astype(jnp.int32)
+        rank = jnp.sum(jnp.where(number == chosen[k], before, 0.0), axis=0, keepdims=True)
+        place_row_ref[k : k + 1, :] = chosen[k] * capacity + rank.astype(jnp.int32)
+        facts[k : k + 1, :] = (chosen[k] * capacity).astype(jnp.float32) + rank
+        facts[topk + k : topk + k + 1, :] = route_ref[k : k + 1, :]
+    facts_col[...] = jnp.transpose(facts[...])
+    gain_row[...] = gain_ref[...].astype(jnp.float32).reshape(1, -1)
 
     odd = chip % 2
     key_lane = (lane // head_size) == odd
@@ -498,6 +500,7 @@
     def chip_step(s, carry):
         number = partner(2 * s) // 2
         near = 2 * number + core
+        push(early + s)
 
         @pl.when(s > 0)
         def _():
@@ -559,7 +562,6 @@
         attended[tp, short:, part] = jnp.where(short_low, even, uneven).astype(jnp.bfloat16)
     direct(0).start()
     direct(1).start()
-    down_copy.start()
 
     def projected(owner):
         return jnp.dot(
@@ -573,6 +575,8 @@
         direct(which).wait_recv()
         relay(which).start()
         mixed = mixed + projected(owner)
+    push(pieces - 1)
+    down_copy.start()
     relay(0).wait_recv()
     relay(1).wait_recv()
     mixed_ref[...] = (mixed + projected((beside + 2) % 4)).astype(mixed_ref.dtype)
@@ -590,11 +594,6 @@
             preferred_element_type=jnp.float32,
         ).astype(jnp.bfloat16)
 
-    first = rows_for(0)
-    full[0, 0] = first[:half]
-    outbox[0, 1] = first[half:]
-    dispatch(0, 1).start()
-
     def fill(i, carry):
         made_rows = rows_for(i)
         outbox[i, 0] = made_rows[:half]
@@ -603,12 +602,18 @@
         dispatch(i, 1).start()
         return carry
 
-    lax.fori_loop(1, groups, fill, 0)
+    lax.fori_loop(2, groups, fill, 0)
+    lax.fori_loop(1, 2, fill, 0)
+    first = rows_for(0)
+    full[0, 0] = first[:half]
+    outbox[0, 1] = first[half:]
+    dispatch(0, 1).start()
     blended[...] = mixed_ref[...].astype(jnp.float32)
     for load in loads:
         load.wait()
-    for copy in weight_copies:
-        copy.wait_recv()
+    for number in range(pieces):
+        for copy in weight_copies(number):
+            copy.wait_recv()
 
     def hidden(i):
         square = jnp.zeros((half, 1), jnp.float32)
@@ -618,7 +623,7 @@
         factor = lax.rsqrt(square / (shards * columns) + NORM_EPS)
         for j in range(shards):
             span = pl.ds(pl.multiple_of(owners[j] * columns, columns), columns)
-            gain = gain_ref[0:1, span].astype(jnp.float32)
+            gain = gain_row[0:1, span]
             wide_rows[:, span] = (full[i, j].astype(jnp.float32) * factor * gain).astype(
                 jnp.bfloat16
             )
@@ -641,24 +646,27 @@
     def step(i, carry):
         @pl.when(i < groups)
         def _():
-            @pl.when(i > 0)
+            b = (i + 2) % groups
+
+            @pl.when(b > 0)
             def _():
-                dispatch(i, 0).wait_recv()
-
-            dispatch(i, 1).wait_recv()
-            exchange(i, full, one_send, one_recv).start()
+                dispatch(b, 0).wait_recv()
+
+            dispatch(b, 1).wait_recv()
+            exchange(b, full, one_send, one_recv).start()
 
         @pl.when((i >= 1) & (i < groups + 1))
         def _():
-            exchange(i - 1, full, one_send, one_recv).wait_recv()
-            hidden(i - 1)
-            exchange(i - 1, act, two_send, two_recv).start()
+            b = (i + 1) % groups
+            exchange(b, full, one_send, one_recv).wait_recv()
+            hidden(b)
+            exchange(b, act, two_send, two_recv).start()
 
         @pl.when((i >= 2) & (i < groups + 2))
         def _():
-            b = i - 2
-
-            @pl.when(b == 0)
+            b = i % groups
+
+            @pl.when(i == 2)
             def _():
                 down_copy.wait_recv()
 
@@ -681,7 +689,7 @@
 
         @pl.when(i >= 3)
         def _():
-            b = i - 3
+            b = (i - 1) % groups
 
             @pl.when(b == 0)
             def _():
@@ -693,14 +701,15 @@
                 arrive_back(b, 1).wait_recv()
 
             numbers = lax.broadcasted_iota(jnp.int32, (rows, capacity), 1) + b * capacity
+            wide_numbers = numbers.astype(jnp.float32)
             added = blended[...]
             rows_back = returned[b].reshape(capacity, columns)
             for k in range(topk):
-                taken = jnp.where(numbers == place_col_ref[:, k : k + 1], 1.0, 0.0)
+                taken = jnp.where(wide_numbers == facts_col[:, k : k + 1], 1.0, 0.0)
                 picked = jnp.dot(
                     taken.astype(jnp.bfloat16), rows_back, preferred_element_type=jnp.float32
                 )
-                added = added + route_ref[:, k : k + 1] * picked
+                added = added + facts_col[:, topk + k : topk + k + 1] * picked
             blended[...] = added
 
         return carry
@@ -746,8 +755,9 @@
         def _():
             answer(n).wait_send()
 
-    for copy in weight_copies:
-        copy.wait_send()
+    for number in range(pieces):
+        for copy in weight_copies(number):
+            copy.wait_send()
 
 
 def layer_fused(
@@ -777,12 +787,14 @@
     return pl.pallas_call(
         functools.partial(layer_kernel, heads, groups),
         out_shape=jax.ShapeDtypeStruct(residual.shape, jnp.bfloat16),
-        in_specs=[pl.BlockSpec(memory_space=pltpu.VMEM)] * 10
+        in_specs=[pl.BlockSpec(memory_space=pltpu.VMEM)] * 9
         + [pl.BlockSpec(memory_space=pl.ANY)] * 3,
         out_specs=pl.BlockSpec(memory_space=pltpu.VMEM),
         scratch_shapes=[
-            pltpu.VMEM(index.shape[::-1], jnp.int32),
             pltpu.VMEM(index.shape, jnp.int32),
+            pltpu.VMEM((8, rows), jnp.float32),
+            pltpu.VMEM((rows, 8), jnp.float32),
+            pltpu.VMEM((1, shards * columns), jnp.float32),
             pltpu.VMEM((rows, columns), jnp.bfloat16),
             pltpu.VMEM((heads, rows, lanes), jnp.bfloat16),
             pltpu.VMEM((heads, rows // 2, lanes), jnp.bfloat16),
@@ -816,8 +828,8 @@
             dma((heads,)),
             dma((4,)),
             dma((4,)),
-            dma((2,)),
-            dma((2,)),
+            dma((8, 2)),
+            dma((8, 2)),
             dma((3,)),
             dma(()),
             dma(()),
@@ -831,7 +843,7 @@
             dma((groups, 2)),
         ],
         compiler_params=pltpu.CompilerParams(
-            collective_id=1, has_side_effects=True, vmem_limit_bytes=60 * 2**20
+            collective_id=1, has_side_effects=True, vmem_limit_bytes=67043328
         ),
     )(
         query_rows,
@@ -840,10 +852,9 @@
         gates,
         output_weight,
         residual,
-        index.T,
         index,
         route_weights,
-        norm_gain.reshape(1, -1),
+        norm_gain,
         gate_weight,
         up_weight,
         down_weight,
@@ -879,7 +890,6 @@
         and heads == 4
         and query_rows.shape[1] == heads * 64
     ):
-        index = expert_index ^ lax.axis_index("sp")
         return layer_fused(
             query_rows,
             key_rows,
@@ -887,8 +897,8 @@
             cum_gates.T,
             output_weight,
             residual,
-            index,
-            route_weights,
+            expert_index.T,
+            route_weights.T,
             norm_gain,
             gate_weight[0],
             up_weight[0],

time: 192 us -> 180 us (0.938)
  Pallas kernels: 185 us -> 177 us
  local copies, waits for them, and re-layouts: 6.21 us -> 1.87 us
    pallas_call x1, Pallas kernels: 185 us -> 177 us  [layer_fused(): pl.pallas_call(functools.partial(layer_kernel, heads, groups), out_shape=...]
    unnamed x3 -> x1, local copies, waits for them, and re-layouts: 4.23 us -> 1.87 us
where the time goes in v3:
time: 180 us; the launch traced here: 179 us
  Pallas kernels  177 us (98%)
  local copies, waits for them, and re-layouts  1.87 us (1%)
    pallas_call x1, Pallas kernels, layer_fused(): pl.pallas_call(functools.partial(layer_kernel, heads, groups), out_shape=...  177 us

profile of v3, /device:TPU:17, one launch (start us, length us, event | category | flops | bytes accessed | tf_op | source)
XLA Modules:
  0.0 178.9 jit_solution(8920033492445638290)
XLA Ops:
  0.0 177.0 %shard_map.118 = bf16[512,512]{1,0:T(8,128)(2,1)} custom-call(bf16[512,256]{1,0:T(8,128)(2,1)} %q_ref.1, bf16[512,256]{1,0:T(8,128)(2,1)} %k_ref.1, bf16[512,256]{1,0:T(8,128)(2,1)} %v_ref.1, f32[4,512]{1,0:T(4,128)} %bitcast.9, bf16[1024,512]{1,0:T(8,128)(2,1)} %weight_ref.1, bf16[512,512]{1,0:T(8,128)(2,1)} %residual_ref.1, s32[2,512]{1,0:T(2,128)} %bitcast.10, ...), custom_call_target="tpu_custom_call" | custom-call | tf_op jit(solution)/shard_map/pallas_call | solution.py:787
  177.0 1.9 %copy.14 = bf16[512,512]{1,0:T(8,128)(2,1)} copy(bf16[512,512]{1,0:T(8,128)(2,1)} %shard_map.118) | data formatting | bytes 1048576

commit v4 on v3

--- a/solution.py
+++ b/solution.py
@@ -575,7 +575,8 @@
         direct(which).wait_recv()
         relay(which).start()
         mixed = mixed + projected(owner)
-    push(pieces - 1)
+    for number in range(early + chips, pieces):
+        push(number)
     down_copy.start()
     relay(0).wait_recv()
     relay(1).wait_recv()
@@ -602,18 +603,19 @@
         dispatch(i, 1).start()
         return carry
 
-    lax.fori_loop(2, groups, fill, 0)
+    def label(n):
+        return 2 * (lax.shift_right_logical(30, 2 * (n // 2)) % chips) + n % 2
+
+    def fill_next(n, carry):
+        return fill(label(n), carry)
+
+    lax.fori_loop(0, groups - 2, fill_next, 0)
     lax.fori_loop(1, 2, fill, 0)
     first = rows_for(0)
     full[0, 0] = first[:half]
     outbox[0, 1] = first[half:]
     dispatch(0, 1).start()
     blended[...] = mixed_ref[...].astype(jnp.float32)
-    for load in loads:
-        load.wait()
-    for number in range(pieces):
-        for copy in weight_copies(number):
-            copy.wait_recv()
 
     def hidden(i):
         square = jnp.zeros((half, 1), jnp.float32)
@@ -646,7 +648,7 @@
     def step(i, carry):
         @pl.when(i < groups)
         def _():
-            b = (i + 2) % groups
+            b = label(i)
 
             @pl.when(b > 0)
             def _():
@@ -655,18 +657,27 @@
             dispatch(b, 1).wait_recv()
             exchange(b, full, one_send, one_recv).start()
 
-        @pl.when((i >= 1) & (i < groups + 1))
-        def _():
-            b = (i + 1) % groups
+        @pl.when((i >= 2) & (i < groups + 2))
+        def _():
+            b = label(i - 2)
+
+            @pl.when(i == 2)
+            def _():
+                for load in loads:
+                    load.wait()
+                for number in range(pieces):
+                    for copy in weight_copies(number):
+                        copy.wait_recv()
+
             exchange(b, full, one_send, one_recv).wait_recv()
             hidden(b)
             exchange(b, act, two_send, two_recv).start()
 
-        @pl.when((i >= 2) & (i < groups + 2))
-        def _():
-            b = i % groups
-
-            @pl.when(i == 2)
+        @pl.when((i >= 4) & (i < groups + 4))
+        def _():
+            b = label(i - 4)
+
+            @pl.when(i == 4)
             def _():
                 down_copy.wait_recv()
 
@@ -687,9 +698,9 @@
                 made[b, 0] = result
                 give_back(b, 0).start()
 
-        @pl.when(i >= 3)
-        def _():
-            b = (i - 1) % groups
+        @pl.when(i >= 6)
+        def _():
+            b = label(i - 6)
 
             @pl.when(b == 0)
             def _():
@@ -714,7 +725,7 @@
 
         return carry
 
-    lax.fori_loop(0, groups + 3, step, 0)
+    lax.fori_loop(0, groups + 6, step, 0)
     out_ref[...] = blended[...].astype(out_ref.dtype)
 
     def settle(i, carry):

time: 180 us -> 168 us (0.933)
  Pallas kernels: 177 us -> 166 us
    pallas_call x1, Pallas kernels: 177 us -> 166 us  [layer_fused(): pl.pallas_call(functools.partial(layer_kernel, heads, groups), out_shape=...]
where the time goes in v4:
time: 168 us
  Pallas kernels  166 us (99%)
  local copies, waits for them, and re-layouts  1.87 us (1%)
    pallas_call x1, Pallas kernels, layer_fused(): pl.pallas_call(functools.partial(layer_kernel, heads, groups), out_shape=...  166 us

profile of v4, /device:TPU:17, one launch (start us, length us, event | category | flops | bytes accessed | tf_op | source)
XLA Modules:
  0.0 168.2 jit_solution(6581094220515736739)
XLA Ops:
  0.0 166.3 %shard_map.118 = bf16[512,512]{1,0:T(8,128)(2,1)} custom-call(bf16[512,256]{1,0:T(8,128)(2,1)} %q_ref.1, bf16[512,256]{1,0:T(8,128)(2,1)} %k_ref.1, bf16[512,256]{1,0:T(8,128)(2,1)} %v_ref.1, f32[4,512]{1,0:T(4,128)} %bitcast.9, bf16[1024,512]{1,0:T(8,128)(2,1)} %weight_ref.1, bf16[512,512]{1,0:T(8,128)(2,1)} %residual_ref.1, s32[2,512]{1,0:T(2,128)} %bitcast.10, ...), custom_call_target="tpu_custom_call" | custom-call | tf_op jit(solution)/shard_map/pallas_call | solution.py:798
  166.3 1.9 %copy.14 = bf16[512,512]{1,0:T(8,128)(2,1)} copy(bf16[512,512]{1,0:T(8,128)(2,1)} %shard_map.118) | data formatting | bytes 1048576

commit v5 on v4

--- a/solution.py
+++ b/solution.py
@@ -698,9 +698,9 @@
                 made[b, 0] = result
                 give_back(b, 0).start()
 
-        @pl.when(i >= 6)
-        def _():
-            b = label(i - 6)
+        @pl.when(i >= 7)
+        def _():
+            b = label(i - 7)
 
             @pl.when(b == 0)
             def _():
@@ -725,7 +725,7 @@
 
         return carry
 
-    lax.fori_loop(0, groups + 6, step, 0)
+    lax.fori_loop(0, groups + 7, step, 0)
     out_ref[...] = blended[...].astype(out_ref.dtype)
 
     def settle(i, carry):

time: 168 us -> 165 us (0.982)
  Pallas kernels: 166 us -> 163 us
    pallas_call x1, Pallas kernels: 166 us -> 163 us  [layer_fused(): pl.pallas_call(functools.partial(layer_kernel, heads, groups), out_shape=...]
where the time goes in v5:
time: 165 us; the launch traced here: 164 us
  Pallas kernels  163 us (99%)
  local copies, waits for them, and re-layouts  1.87 us (1%)
    pallas_call x1, Pallas kernels, layer_fused(): pl.pallas_call(functools.partial(layer_kernel, heads, groups), out_shape=...  163 us

profile of v5, /device:TPU:17, one launch (start us, length us, event | category | flops | bytes accessed | tf_op | source)
XLA Modules:
  0.0 164.4 jit_solution(2776561232594252122)
XLA Ops:
  0.0 162.5 %shard_map.118 = bf16[512,512]{1,0:T(8,128)(2,1)} custom-call(bf16[512,256]{1,0:T(8,128)(2,1)} %q_ref.1, bf16[512,256]{1,0:T(8,128)(2,1)} %k_ref.1, bf16[512,256]{1,0:T(8,128)(2,1)} %v_ref.1, f32[4,512]{1,0:T(4,128)} %bitcast.9, bf16[1024,512]{1,0:T(8,128)(2,1)} %weight_ref.1, bf16[512,512]{1,0:T(8,128)(2,1)} %residual_ref.1, s32[2,512]{1,0:T(2,128)} %bitcast.10, ...), custom_call_target="tpu_custom_call" | custom-call | tf_op jit(solution)/shard_map/pallas_call | solution.py:798
  162.5 1.9 %copy.14 = bf16[512,512]{1,0:T(8,128)(2,1)} copy(bf16[512,512]{1,0:T(8,128)(2,1)} %shard_map.118) | data formatting | bytes 1048576

commit v6 on v5

--- a/solution.py
+++ b/solution.py
@@ -128,19 +128,24 @@
 def layer_kernel(
     heads,
     groups,
-    q_ref,
-    k_ref,
-    v_ref,
     gates_ref,
-    weight_ref,
-    residual_ref,
     index_ref,
     route_ref,
     gain_ref,
+    q_source,
+    k_source,
+    v_source,
+    weight_source,
+    residual_source,
     gate_ref,
     up_ref,
     down_ref,
     out_ref,
+    q_ref,
+    k_ref,
+    v_ref,
+    weight_ref,
+    residual_ref,
     place_row_ref,
     facts,
     facts_col,
@@ -334,7 +339,16 @@
 
     loads = []
     for n, (src, dst) in enumerate(
-        ((gate_ref, gate_all.at[0]), (up_ref, up_all.at[0]), (down_ref, down_all.at[0]))
+        (
+            (q_source, q_ref),
+            (k_source, k_ref),
+            (v_source, v_ref),
+            (weight_source, weight_ref),
+            (residual_source, residual_ref),
+            (gate_ref, gate_all.at[0]),
+            (up_ref, up_all.at[0]),
+            (down_ref, down_all.at[0]),
+        )
     ):
         loads.append(pltpu.make_async_copy(src, dst, load_sem.at[n]))
     for load in loads:
@@ -385,6 +399,8 @@
     for number in range(early):
         push(number)
 
+    for load in loads[:3]:
+        load.wait()
     lane = lax.broadcasted_iota(jnp.int32, (rows, lanes), 1)
     low = lane < head_size
     short = rows // 2
@@ -570,6 +586,8 @@
             preferred_element_type=jnp.float32,
         )
 
+    for load in loads[3:5]:
+        load.wait()
     mixed = residual_ref[...].astype(jnp.float32) + projected(tp)
     for which, owner in ((0, beside), (1, across)):
         direct(which).wait_recv()
@@ -663,7 +681,7 @@
 
             @pl.when(i == 2)
             def _():
-                for load in loads:
+                for load in loads[5:]:
                     load.wait()
                 for number in range(pieces):
                     for copy in weight_copies(number):
@@ -798,10 +816,15 @@
     return pl.pallas_call(
         functools.partial(layer_kernel, heads, groups),
         out_shape=jax.ShapeDtypeStruct(residual.shape, jnp.bfloat16),
-        in_specs=[pl.BlockSpec(memory_space=pltpu.VMEM)] * 9
-        + [pl.BlockSpec(memory_space=pl.ANY)] * 3,
+        in_specs=[pl.BlockSpec(memory_space=pltpu.VMEM)] * 4
+        + [pl.BlockSpec(memory_space=pl.ANY)] * 8,
         out_specs=pl.BlockSpec(memory_space=pltpu.VMEM),
         scratch_shapes=[
+            pltpu.VMEM((rows, width), jnp.bfloat16),
+            pltpu.VMEM((rows, width), jnp.bfloat16),
+            pltpu.VMEM((rows, width), jnp.bfloat16),
+            pltpu.VMEM(output_weight.shape, jnp.bfloat16),
+            pltpu.VMEM(residual.shape, jnp.bfloat16),
             pltpu.VMEM(index.shape, jnp.int32),
             pltpu.VMEM((8, rows), jnp.float32),
             pltpu.VMEM((rows, 8), jnp.float32),
@@ -841,7 +864,7 @@
             dma((4,)),
             dma((8, 2)),
             dma((8, 2)),
-            dma((3,)),
+            dma((8,)),
             dma(()),
             dma(()),
             dma((groups, 2)),
@@ -857,15 +880,15 @@
             collective_id=1, has_side_effects=True, vmem_limit_bytes=67043328
         ),
     )(
+        gates,
+        index,
+        route_weights,
+        norm_gain,
         query_rows,
         key_rows,
         value_rows,
-        gates,
         output_weight,
         residual,
-        index,
-        route_weights,
-        norm_gain,
         gate_weight,
         up_weight,
         down_weight,

time: 165 us -> 164 us (level)
  no operation moved by 1% of the time
where the time goes in v6:
time: 164 us; the launch traced here: 163 us
  Pallas kernels  162 us (99%)
  local copies, waits for them, and re-layouts  1.87 us (1%)
    pallas_call x1, Pallas kernels, layer_fused(): pl.pallas_call(functools.partial(layer_kernel, heads, groups), out_shape=...  162 us

profile of v6, /device:TPU:17, one launch (start us, length us, event | category | flops | bytes accessed | tf_op | source)
XLA Modules:
  0.0 163.4 jit_solution(12737091444034967277)
XLA Ops:
  0.0 161.5 %shard_map.118 = bf16[512,512]{1,0:T(8,128)(2,1)} custom-call(f32[4,512]{1,0:T(4,128)} %bitcast.9, s32[2,512]{1,0:T(2,128)} %bitcast.10, f32[2,512]{1,0:T(2,128)} %bitcast.11, bf16[2048]{0:T(1024)(128)(2,1)} %gain_ref.1, bf16[512,256]{1,0:T(8,128)(2,1)} %q_source.1, bf16[512,256]{1,0:T(8,128)(2,1)} %k_source.1, bf16[512,256]{1,0:T(8,128)(2,1)} %v_source.1, ...), custom_call_target="tpu_custom_call" | custom-call | tf_op jit(solution)/shard_map/pallas_call | solution.py:816
  161.5 1.9 %copy.14 = bf16[512,512]{1,0:T(8,128)(2,1)} copy(bf16[512,512]{1,0:T(8,128)(2,1)} %shard_map.118) | data formatting | bytes 1048576
